TPU v7x, 32 devices: a whole 2x2x4 slice. The times are simulated.
32 devices in a mesh: dp: 4 (over y, x), kv: 4 (over z), tp: 2 (over core).
Axes of the slice: x: 2, y: 2, z: 4, core: 2. Of those that a mesh axis runs over, the one named last changes fastest.
Arguments:
- tokens: bfloat16 [96, 4096], P('dp', ('kv', 'tp')), may hold values from -10 to 10
- gain_mixer: bfloat16 [4096], replicated, may hold values from 0.099609375 to 1.8984375
- weight_query: bfloat16 [4096, 16, 128], P('kv', 'tp'), may hold values from -0.09375 to 0.09375
- weight_key: bfloat16 [4096, 16, 128], P('kv', 'tp'), may hold values from -0.09375 to 0.09375
- weight_value: bfloat16 [4096, 16, 128], P('kv', 'tp'), may hold values from -0.09375 to 0.09375
- weight_outgate: bfloat16 [4096, 16, 128], P('kv', 'tp'), may hold values from -0.09375 to 0.09375
- weight_ingate: bfloat16 [4096, 16], replicated, may hold values from -0.09375 to 0.09375
- weight_forget: bfloat16 [4096, 16], replicated, may hold values from -0.09375 to 0.09375
- bias_input: float32 [16], replicated, may hold values from -3 to 3
- bias_forget: float32 [16], replicated, may hold values from 0 to 5
- memory: float32 [96, 16, 128, 128], P(('dp', 'kv'), 'tp'), may hold values from -2.5 to 2.5
- normalizer: float32 [96, 16, 128], P(('dp', 'kv'), 'tp'), may hold values from -2.5 to 2.5
- stabilizer: float32 [96, 16], P(('dp', 'kv'), 'tp'), may hold values from -1 to 3
- head_gain: bfloat16 [16, 128], replicated, may hold values from 0.099609375 to 1.8984375
- weight_out: bfloat16 [2048, 4096], P('tp', 'kv'), may hold values from -0.125 to 0.125
- gain_channel: bfloat16 [4096], replicated, may hold values from 0.099609375 to 1.8984375
- weight_up: bfloat16 [4096, 16384], P(None, ('kv', 'tp')), may hold values from -0.09375 to 0.09375
- weight_down: bfloat16 [16384, 4096], P(('kv', 'tp')), may hold values from -0.0625 to 0.0625
Outputs:
- layer_out: bfloat16 [96, 4096], P('dp', ('kv', 'tp'))
- new_memory: float32 [96, 16, 128, 128], P(('dp', 'kv'), 'tp')
- new_normalizer: float32 [96, 16, 128], P(('dp', 'kv'), 'tp')
- new_stabilizer: float32 [96, 16], P(('dp', 'kv'), 'tp')
All inputs are finite; a program needn't handle non-finite values.
Results may differ from a plain program's by a relative error of at most 0.017.
Values may be sent and summed in bfloat16 or wider, within the bound.
No kernel may reach another device: no remote copies, remote signals or barrier semaphores. Data moves between devices by JAX's collectives and lax.ppermute only.
A program may use at most 128 MiB of HBM per device.

v0:
```python
import jax
import jax.numpy as jnp
from jax import lax
from jax.sharding import PartitionSpec as P

epsilon = 1e-06


def project(scaled, weight):
    return jnp.dot(scaled, weight.reshape(weight.shape[0], -1), preferred_element_type=jnp.float32)


def scale_slab(slab_rows, gain, offset):
    rows_wide = slab_rows.astype(jnp.float32)
    gain_slice = lax.dynamic_slice_in_dim(gain, offset, slab_rows.shape[1], 0).astype(jnp.float32)
    return ((rows_wide * gain_slice).astype(jnp.bfloat16), jnp.sum(rows_wide * rows_wide, axis=1))


def cell_update(
    queries,
    keys_in,
    values_in,
    outgates,
    ingate,
    forget,
    memory,
    normalizer,
    stabilizer,
    head_scale,
):
    head_dim = queries.shape[-1]
    query_wide = queries.astype(jnp.float32)
    key_scaled = keys_in.astype(jnp.float32) * head_dim ** (-0.5)
    value_wide = values_in.astype(jnp.float32)
    new_stabilizer = jnp.maximum(forget + stabilizer, ingate)
    retain = jnp.exp(forget + stabilizer - new_stabilizer)
    inflow = jnp.exp(ingate - new_stabilizer)
    new_memory = (
        retain[..., None, None] * memory
        + (inflow[..., None] * value_wide)[..., :, None] * key_scaled[..., None, :]
    )
    new_normalizer = retain[..., None] * normalizer + inflow[..., None] * key_scaled
    numerator = jnp.einsum("bhvk,bhk->bhv", new_memory, query_wide, precision=lax.Precision.HIGHEST)
    denominator = jnp.sum(new_normalizer * query_wide, axis=-1)
    readout = numerator / jnp.maximum(jnp.abs(denominator), jnp.exp(-new_stabilizer))[..., None]
    centered = readout - jnp.mean(readout, axis=-1, keepdims=True)
    normed = centered * lax.rsqrt(jnp.mean(centered * centered, axis=-1, keepdims=True) + epsilon)
    gated_out = (
        normed * head_scale.astype(jnp.float32) * jax.nn.sigmoid(outgates.astype(jnp.float32))
    )
    return (gated_out.astype(jnp.bfloat16), new_memory, new_normalizer, new_stabilizer)


def body(
    tokens,
    gain_mixer,
    weight_query,
    weight_key,
    weight_value,
    weight_outgate,
    weight_ingate,
    weight_forget,
    bias_input,
    bias_forget,
    memory,
    normalizer,
    stabilizer,
    head_gain,
    weight_out,
    gain_channel,
    weight_up,
    weight_down,
):
    kv_rank = lax.axis_index("kv")
    tp_rank = lax.axis_index("tp")
    own_rows = memory.shape[0]
    heads_here = memory.shape[1]
    head_dim = memory.shape[2]
    width_full = gain_mixer.shape[0]
    head_start = tp_rank * heads_here
    gate_weights = jnp.concatenate(
        [
            lax.dynamic_slice_in_dim(weight_ingate, head_start, heads_here, 1),
            lax.dynamic_slice_in_dim(weight_forget, head_start, heads_here, 1),
        ],
        axis=1,
    )
    slab_rows = lax.all_gather(tokens, "tp", axis=1, tiled=True)
    slab_cols = slab_rows.shape[1]
    head_view = (own_rows, heads_here, head_dim)
    col_start = kv_rank * slab_cols
    scaled, squares = scale_slab(slab_rows, gain_mixer, col_start)
    partials = [
        project(scaled, weight)
        for weight in (weight_query, weight_key, weight_value, weight_outgate)
    ]
    gate_part = jnp.dot(
        scaled,
        lax.dynamic_slice_in_dim(gate_weights, col_start, slab_cols, 0),
        preferred_element_type=jnp.float32,
    )
    summed = (
        lax.psum_scatter(
            partials[0].astype(jnp.bfloat16), "kv", scatter_dimension=0, tiled=True
        ).astype(jnp.float32),
        lax.psum_scatter(
            partials[1].astype(jnp.bfloat16), "kv", scatter_dimension=0, tiled=True
        ).astype(jnp.float32),
        lax.psum_scatter(
            partials[2].astype(jnp.bfloat16), "kv", scatter_dimension=0, tiled=True
        ).astype(jnp.float32),
        lax.psum_scatter(
            partials[3].astype(jnp.bfloat16), "kv", scatter_dimension=0, tiled=True
        ).astype(jnp.float32),
        lax.psum_scatter(
            gate_part.astype(jnp.bfloat16), "kv", scatter_dimension=0, tiled=True
        ).astype(jnp.float32),
        lax.psum_scatter(
            squares.astype(jnp.bfloat16), "kv", scatter_dimension=0, tiled=True
        ).astype(jnp.float32),
    )
    own_squares = summed[5]
    inverse = lax.rsqrt(own_squares / width_full + epsilon)[:, None]
    queries = (inverse * summed[0]).astype(jnp.bfloat16).reshape(head_view)
    keys_proj = (inverse * summed[1]).astype(jnp.bfloat16).reshape(head_view)
    values_proj = (inverse * summed[2]).astype(jnp.bfloat16).reshape(head_view)
    outgates = (inverse * summed[3]).astype(jnp.bfloat16).reshape(head_view)
    gate_pre = inverse * summed[4]
    ingate = gate_pre[:, :heads_here] + lax.dynamic_slice_in_dim(
        bias_input, head_start, heads_here, 0
    )
    forget = jax.nn.log_sigmoid(
        gate_pre[:, heads_here:] + lax.dynamic_slice_in_dim(bias_forget, head_start, heads_here, 0)
    )
    head_scale = lax.dynamic_slice_in_dim(head_gain, head_start, heads_here, 0)
    heads_out, new_memory, new_normalizer, new_stabilizer = cell_update(
        queries,
        keys_proj,
        values_proj,
        outgates,
        ingate,
        forget,
        memory,
        normalizer,
        stabilizer,
        head_scale,
    )
    heads_flat = heads_out.reshape(own_rows, heads_here * head_dim)
    partial_out = jnp.dot(
        lax.all_gather(heads_flat, "kv", axis=0, tiled=True),
        weight_out,
        preferred_element_type=jnp.float32,
    ).astype(jnp.bfloat16)
    partial_wide = lax.optimization_barrier(partial_out).astype(jnp.float32)
    projected = lax.psum_scatter(
        partial_wide.astype(jnp.bfloat16), "tp", scatter_dimension=1, tiled=True
    ).astype(jnp.float32)
    mixed_rows = (tokens.astype(jnp.float32) + projected).astype(jnp.bfloat16)
    scaled_mlp, squares_mlp = scale_slab(
        lax.all_gather(mixed_rows, ("kv", "tp"), axis=1, tiled=True), gain_channel, jnp.int32(0)
    )
    weight_block = weight_up
    up_total = jnp.dot(scaled_mlp, weight_block, preferred_element_type=jnp.float32)
    inverse_mlp = lax.rsqrt(squares_mlp / width_full + epsilon)[:, None]
    activation = jax.nn.relu(inverse_mlp * up_total)
    squared = (activation * activation).astype(jnp.bfloat16)
    weight_block = weight_down
    transposed = lax.psum_scatter(
        jnp.einsum("uc,ru->cr", weight_block, squared, preferred_element_type=jnp.float32),
        ("kv", "tp"),
        scatter_dimension=0,
        tiled=True,
    )
    layer_out = (mixed_rows.astype(jnp.float32) + transposed.T).astype(jnp.bfloat16)
    return (layer_out, new_memory, new_normalizer, new_stabilizer)


def solution(mesh):
    placed = (
        P("dp", ("kv", "tp")),
        P(),
        P("kv", "tp", None),
        P("kv", "tp", None),
        P("kv", "tp", None),
        P("kv", "tp", None),
        P(),
        P(),
        P(),
        P(),
        P(("dp", "kv"), "tp", None, None),
        P(("dp", "kv"), "tp", None),
        P(("dp", "kv"), "tp"),
        P(),
        P("tp", "kv"),
        P(),
        P(None, ("kv", "tp")),
        P(("kv", "tp"), None),
    )
    return jax.shard_map(
        body,
        mesh=mesh,
        in_specs=placed,
        out_specs=(
            P("dp", ("kv", "tp")),
            P(("dp", "kv"), "tp", None, None),
            P(("dp", "kv"), "tp", None),
            P(("dp", "kv"), "tp"),
        ),
        check_vma=False,
    )
```

profile of v0, /device:TPU:0, one launch (start us, length us, event | category | flops | bytes accessed | tf_op | source)
XLA Modules:
  0.0 150.9 jit_solution(1594362758720483900)
XLA Ops:
  7.2 2.3 %all_gather.9 = bf16[24,1024]{1,0:T(8,128)(2,1)S(1)} all-gather(bf16[24,512]{1,0:T(8,128)(2,1)} %param.18), channel_id=1, replica_groups=mesh['dp'=4,'kv'=4,'tp'=2] {'tp'}, dimensions={1}, use_global_device_ids=true | all-gather | bytes 73728 | tf_op jit(solution)/shard_map/all_gather | solution.py:88
  9.6 0.8 dynamic-slice_convert_fusion.1
  10.4 2.1 %fusion.19 = bf16[24,1024]{1,0:T(8,128)(2,1)S(1)} fusion(bf16[128,8,8,128]{3,2,1,0:T(8,128)(2,1)} %bitcast.73, bf16[24,1024]{1,0:T(8,128)(2,1)S(1)} %all_gather.9, f32[1024]{0:T(1024)S(1)} %dynamic-slice_convert_fusion.1), kind=kOutput, calls=%fused_computation.18 | convolution fusion | flops 50429952 | bytes 2199552 | tf_op jit(solution)/shard_map/dot_general | solution.py:10
  12.5 0.4 fusion.22
  13.0 0.4 fusion.25
  13.4 0.8 copy-done.13
  14.2 0.4 fusion.28
  14.6 17.0 %fusion.61 = (bf16[8,1024]{1,0:T(8,128)(2,1)S(1)}, bf16[8,1024]{1,0:T(8,128)(2,1)S(1)}, bf16[8,1024]{1,0:T(8,128)(2,1)S(1)}, bf16[8,1024]{1,0:T(8,128)(2,1)S(1)}) fusion(bf16[24,1024]{1,0:T(8,128)(2,1)S(1)} %fusion.28, bf16[24,1024]{1,0:T(8,128)(2,1)S(1)} %fusion.22, bf16[24,1024]{1,0:T(8,128)(2,1)S(1)} %fusion.19, bf16[24,1024]{1,0:T(8,128)(2,1)S(1)} %fusion.25), kind=kCustom, calls=%all-reduce-scatter.4 | all-reduce-scatter fusion | flops 131073 | bytes 262656
  31.6 1.3 collective-permute-start.2
  32.9 1.8 %collective-permute-start = (bf16[6,1024]{1,0:T(8,128)(2,1)S(1)}, bf16[6,1024]{1,0:T(8,128)(2,1)S(1)}, u32[]{:S(2)}, u32[]{:S(2)}) collective-permute-start(bf16[6,1024]{1,0:T(8,128)(2,1)S(1)} %slice.8), channel_id=1, source_target_pairs={{0,2},{2,4},{4,6},{1,3},{3,5},{5,7},{8,10},{10,12},{12,14},{9,11},... | collective-permute-start | bytes 36872
  34.7 3.5 %collective-permute-start.1 = (bf16[6,1024]{1,0:T(8,128)(2,1)S(1)}, bf16[6,1024]{1,0:T(8,128)(2,1)S(1)}, u32[]{:S(2)}, u32[]{:S(2)}) collective-permute-start(bf16[6,1024]{1,0:T(8,128)(2,1)S(1)} %slice.9), channel_id=1, source_target_pairs={{0,2},{2,4},{4,6},{1,3},{3,5},{5,7},{8,10},{10,12},{12,14},{9,11},... | collective-permute-start | bytes 36872
  38.2 1.9 %collective-permute-start.3 = (bf16[6,1024]{1,0:T(8,128)(2,1)S(1)}, bf16[6,1024]{1,0:T(8,128)(2,1)S(1)}, u32[]{:S(2)}, u32[]{:S(2)}) collective-permute-start(bf16[6,1024]{1,0:T(8,128)(2,1)S(1)} %slice.11), channel_id=1, source_target_pairs={{0,2},{2,4},{4,6},{1,3},{3,5},{5,7},{8,10},{10,12},{12,14},{9,11},... | collective-permute-start | bytes 36872
  40.4 0.6 fusion.64
  41.0 0.1 convolution_convert_fusion.1
  41.8 8.5 %all-reduce.10 = (bf16[24]{0:T(256)(128)(2,1)S(1)}, bf16[24,16]{1,0:T(8,128)(2,1)S(1)}) all-reduce(bf16[24]{0:T(256)(128)(2,1)S(1)} %fusion.37, bf16[24,16]{1,0:T(8,128)(2,1)S(1)} %convolution_convert_fusion.1), channel_id=2, replica_groups=mesh['dp'=4,'kv'=4,'tp'=2] {'kv'}, use_global_device_ids=true, to_apply=%region_1.0.clone | all-reduce | flops 408 | bytes 1632
  51.5 0.1 concatenate.4
  51.7 0.1 concatenate.5
  52.1 0.7 multiply_reduce_fusion.1
  52.9 2.5 %multiply_add_fusion = f32[6,8,128,128]{3,2,1,0:T(8,128)S(1)} fusion(f32[6,8,128,128]{3,2,1,0:T(8,128)} %param.28, f32[6,8,128]{2,1,0:T(8,128)S(1)} %get-tuple-element.19, f32[6,8,128]{2,1,0:T(8,128)S(1)} %bitcast_multiply_fusion.3, f32[6,8]{1,0:T(8,128)S(1)} %subtract_exponential_fusion.1), kind=kLoop, calls=%fused_computation.1 | loop fusion | flops 2359296 | bytes 6340800 | tf_op jit(solution)/shard_map/add | solution.py:39
  55.4 1.7 %copy-done.1 = f32[6,8,128,128]{3,2,1,0:T(8,128)} copy-done((f32[6,8,128,128]{3,2,1,0:T(8,128)}, f32[6,8,128,128]{3,2,1,0:T(8,128)S(1)}, u32[]{:S(2)}) %copy-start.1) | copy-done | bytes 3145752
  57.0 2.5 %fusion.65 = f32[6,8,1,128]{3,2,1,0:T(1,128)S(1)} fusion(f32[6,8,128,128]{3,2,1,0:T(8,128)S(1)} %multiply_add_fusion, bf16[6,8,128,1]{2,3,1,0:T(2,128)(2,1)S(1)} %reshape.93), kind=kOutput, calls=%fused_computation.83 | convolution fusion | flops 9437184 | bytes 3182592 | tf_op jit(solution)/shard_map/bhvk,bhk->bhv/dot_general | solution.py:43
  59.6 0.2 fusion.60
  59.7 0.2 multiply_reduce_fusion
  60.1 13.1 %all-gather = bf16[4,6,1024]{2,1,0:T(8,128)(2,1)S(1)} all-gather(bf16[1,6,1024]{2,1,0:T(8,128)(2,1)S(1)} %reshape.87), channel_id=1, replica_groups=mesh['dp'=4,'kv'=4,'tp'=2] {'kv'}, dimensions={0}, use_global_device_ids=true | all-gather | bytes 61440 | tf_op jit(solution)/shard_map/all_gather | solution.py:150
  73.3 1.0 convolution_convert_fusion
  74.4 7.3 %reduce-scatter.11.cloned.1.call-done = bf16[24,512]{1,0:T(8,128)(2,1)} async-done(((bf16[24,1024]{1,0:T(8,128)(2,1)}), bf16[24,512]{1,0:T(8,128)(2,1)}) %reduce-scatter.11.cloned.1.call-update) | async-done | bytes 24592 | tf_op jit(solution)/shard_map/reduce_scatter | solution.py:155
  81.6 0.7 add_convert_fusion
  82.4 14.3 %all_gather.11 = bf16[24,4096]{1,0:T(8,128)(2,1)S(1)} all-gather(bf16[24,512]{1,0:T(8,128)(2,1)S(1)} %add_convert_fusion), channel_id=1, replica_groups=mesh['dp'=4,'kv'=4,'tp'=2] {'kv','tp'}, dimensions={1}, use_global_device_ids=true | all-gather | bytes 221184 | tf_op jit(solution)/shard_map/all_gather | solution.py:160
  96.7 0.2 fusion.31
  96.9 13.6 %convolution_bitcast_fusion = f32[4096,24]{0,1:T(8,128)} fusion(bf16[2048,4096]{1,0:T(8,128)(2,1)} %param.35, bf16[4096,2048]{1,0:T(8,128)(2,1)} %param.34, bf16[24,4096]{1,0:T(8,128)(2,1)S(1)} %all_gather.11, f32[4096]{0:T(1024)S(1)} %convert_element_type.155, f32[24]{0:T(128)S(1)} %add_rsqrt_fusion.1), kind=kOutput, calls=%fused_computation | convolution fusion | flops 805797888 | bytes 34160736 | tf_op jit(solution)/shard_map/uc,ru->cr/dot_general | solution.py:169
  110.6 32.1 %reduce-scatter.13.cloned.1.call-done = f32[512,24]{0,1:T(8,128)} async-done(((f32[4096,24]{0,1:T(8,128)}), f32[512,24]{0,1:T(8,128)}) %reduce-scatter.13.cloned.1.call-update) | async-done | bytes 49168 | tf_op jit(solution)/shard_map/reduce_scatter | solution.py:168
  142.7 1.4 fusion.41
  (64 shorter events, 1.5 us)
Async XLA Ops:
  7.2 66.1 %copy-start = (bf16[1024,1024]{1,0:T(8,128)(2,1)S(1)}, bf16[1024,1024]{1,0:T(8,128)(2,1)}, u32[]{:S(2)}) copy-start(bf16[1024,1024]{1,0:T(8,128)(2,1)} %param.32) | copy-start | bytes 6291460
  7.2 74.5 %reduce-scatter.11.cloned.1.call-start = ((), (), s32[]{:S(2)}) async-start(), calls=%async_computation.2 | async-start | bytes 73728 | tf_op jit(solution)/shard_map/reduce_scatter | solution.py:155
  9.6 3.0 %copy-start.11 = (bf16[1024,8,128]{2,1,0:T(8,128)(2,1)S(1)}, bf16[1024,8,128]{2,1,0:T(8,128)(2,1)}, u32[]{:S(2)}) copy-start(bf16[1024,8,128]{2,1,0:T(8,128)(2,1)} %param.21) | copy-start | bytes 6291460
  10.4 2.5 %copy-start.12 = (bf16[1024,8,128]{2,1,0:T(8,128)(2,1)S(1)}, bf16[1024,8,128]{2,1,0:T(8,128)(2,1)}, u32[]{:S(2)}) copy-start(bf16[1024,8,128]{2,1,0:T(8,128)(2,1)} %param.20) | copy-start | bytes 6291460
  12.5 1.7 %copy-start.13 = (bf16[1024,8,128]{2,1,0:T(8,128)(2,1)S(1)}, bf16[1024,8,128]{2,1,0:T(8,128)(2,1)}, u32[]{:S(2)}) copy-start(bf16[1024,8,128]{2,1,0:T(8,128)(2,1)} %param.23) | copy-start | bytes 6291460
  12.9 27.3 %copy-start.14 = (f32[16]{0:T(128)S(1)}, f32[16]{0:T(128)}, u32[]{:S(2)}) copy-start(f32[16]{0:T(128)} %param.27) | copy-start | bytes 196
  12.9 27.4 %copy-start.15 = (f32[16]{0:T(128)S(1)}, f32[16]{0:T(128)}, u32[]{:S(2)}) copy-start(f32[16]{0:T(128)} %param.26) | copy-start | bytes 196
  13.0 27.4 %copy-start.9 = (u32[32]{0:T(128)S(1)}, u32[32]{0:T(128)}, u32[]{:S(2)}) copy-start(u32[32]{0:T(128)} %constant.47) | copy-start | bytes 388
  13.0 28.0 %copy-start.4 = (bf16[4096,16]{0,1:T(8,128)(2,1)S(1)}, bf16[4096,16]{0,1:T(8,128)(2,1)}, u32[]{:S(2)}) copy-start(bf16[4096,16]{0,1:T(8,128)(2,1)} %param.25) | copy-start | bytes 393220
  13.0 28.0 %copy-start.5 = (bf16[4096,16]{0,1:T(8,128)(2,1)S(1)}, bf16[4096,16]{0,1:T(8,128)(2,1)}, u32[]{:S(2)}) copy-start(bf16[4096,16]{0,1:T(8,128)(2,1)} %param.24) | copy-start | bytes 393220
  13.4 37.1 %copy-start.7 = (f32[6,8]{1,0:T(8,128)S(1)}, f32[6,8]{1,0:T(8,128)}, u32[]{:S(2)}) copy-start(f32[6,8]{1,0:T(8,128)} %param.30) | copy-start | bytes 580
  13.4 37.3 %copy-start.10 = (bf16[16,128]{1,0:T(8,128)(2,1)S(1)}, bf16[16,128]{1,0:T(8,128)(2,1)}, u32[]{:S(2)}) copy-start(bf16[16,128]{1,0:T(8,128)(2,1)} %param.31) | copy-start | bytes 12292
  13.4 38.7 %copy-start.6 = (f32[6,8,128]{2,1,0:T(8,128)S(1)}, f32[6,8,128]{2,1,0:T(8,128)}, u32[]{:S(2)}) copy-start(f32[6,8,128]{2,1,0:T(8,128)} %param.29) | copy-start | bytes 73732
  31.6 19.8 %collective-permute-start.2 = (bf16[6,1024]{1,0:T(8,128)(2,1)S(1)}, bf16[6,1024]{1,0:T(8,128)(2,1)S(1)}, u32[]{:S(2)}, u32[]{:S(2)}) collective-permute-start(bf16[6,1024]{1,0:T(8,128)(2,1)S(1)} %slice.10), channel_id=1, source_target_pairs={{0,2},{2,4},{4,6},{1,3},{3,5},{5,7},{8,10},{10,12},{12,14},{9,11},... | collective-permute-start | bytes 36872
  32.9 18.6 %collective-permute-start = (bf16[6,1024]{1,0:T(8,128)(2,1)S(1)}, bf16[6,1024]{1,0:T(8,128)(2,1)S(1)}, u32[]{:S(2)}, u32[]{:S(2)}) collective-permute-start(bf16[6,1024]{1,0:T(8,128)(2,1)S(1)} %slice.8), channel_id=1, source_target_pairs={{0,2},{2,4},{4,6},{1,3},{3,5},{5,7},{8,10},{10,12},{12,14},{9,11},... | collective-permute-start | bytes 36872
  34.7 17.0 %collective-permute-start.1 = (bf16[6,1024]{1,0:T(8,128)(2,1)S(1)}, bf16[6,1024]{1,0:T(8,128)(2,1)S(1)}, u32[]{:S(2)}, u32[]{:S(2)}) collective-permute-start(bf16[6,1024]{1,0:T(8,128)(2,1)S(1)} %slice.9), channel_id=1, source_target_pairs={{0,2},{2,4},{4,6},{1,3},{3,5},{5,7},{8,10},{10,12},{12,14},{9,11},... | collective-permute-start | bytes 36872
  38.2 13.6 %collective-permute-start.3 = (bf16[6,1024]{1,0:T(8,128)(2,1)S(1)}, bf16[6,1024]{1,0:T(8,128)(2,1)S(1)}, u32[]{:S(2)}, u32[]{:S(2)}) collective-permute-start(bf16[6,1024]{1,0:T(8,128)(2,1)S(1)} %slice.11), channel_id=1, source_target_pairs={{0,2},{2,4},{4,6},{1,3},{3,5},{5,7},{8,10},{10,12},{12,14},{9,11},... | collective-permute-start | bytes 36872
  50.6 4.7 %copy-start.3 = (f32[6,8]{1,0:T(8,128)}, f32[6,8]{1,0:T(8,128)S(1)}, u32[]{:S(2)}) copy-start(f32[6,8]{1,0:T(8,128)S(1)} %get-tuple-element.18) | copy-start | bytes 580
  55.4 1.7 %copy-start.1 = (f32[6,8,128,128]{3,2,1,0:T(8,128)}, f32[6,8,128,128]{3,2,1,0:T(8,128)S(1)}, u32[]{:S(2)}) copy-start(f32[6,8,128,128]{3,2,1,0:T(8,128)S(1)} %multiply_add_fusion) | copy-start | bytes 9437188
  59.6 14.8 %copy-start.8 = (bf16[4096]{0:T(1024)(128)(2,1)S(1)}, bf16[4096]{0:T(1024)(128)(2,1)}, u32[]{:S(2)}) copy-start(bf16[4096]{0:T(1024)(128)(2,1)} %param.33) | copy-start | bytes 24580
  59.6 22.1 %copy-start.2 = (bf16[24,512]{1,0:T(8,128)(2,1)S(1)}, bf16[24,512]{1,0:T(8,128)(2,1)}, u32[]{:S(2)}) copy-start(bf16[24,512]{1,0:T(8,128)(2,1)} %param.18) | copy-start | bytes 73732
  74.3 68.4 %reduce-scatter.13.cloned.1.call-start = ((), (), s32[]{:S(2)}) async-start(), calls=%async_computation.3 | async-start | bytes 442368 | tf_op jit(solution)/shard_map/reduce_scatter | solution.py:168
Sparse Core Ops, SparseCore 0:
  74.4 7.1 reduce-scatter.10
  110.7 31.9 reduce-scatter.12
where the time goes:
time: 151 us
  blocking collectives  55.3 us (37%)
  waiting for transfers between devices  39.4 us (26%)
  matrix products  20.6 us (14%)
  between operations  15.7 us (10%)
  starting transfers between devices  8.52 us (6%)
  other arithmetic  7.41 us (5%)
  local copies, waits for them, and re-layouts  3.9 us (3%)
    reduce_scatter x1, waiting for transfers between devices, body(): lax.psum_scatter(jnp.einsum('uc,ru->cr', weight_block, squared, preferred...  32.1 us
    unnamed x2, blocking collectives  25.5 us
    all_gather x1, blocking collectives, body(): lax.all_gather(mixed_rows, ('kv', 'tp'), axis=1, tiled=True)  14.3 us
    dot_general x1, matrix products, body(): jnp.einsum('uc,ru->cr', weight_block, squared, preferred_element_type=jnp...  13.6 us
    all_gather x1, blocking collectives, body(): lax.all_gather(heads_flat, 'kv', axis=0, tiled=True)  13.1 us
    unnamed x4, starting transfers between devices  8.44 us
    reduce_scatter x1, waiting for transfers between devices, body(): lax.psum_scatter(partial_wide.astype(jnp.bfloat16), 'tp', scatter_dimensi...  7.28 us
    unnamed x43, local copies, waits for them, and re-layouts  3.71 us
  transfers between devices with their start and end apart: 6, of which 2 were waited for; matrix products, arithmetic and copies ran while one was open for 1% of the time, Pallas kernels for 0%

commit v1 on v0

v1 whole, which is shorter than its diff:
```python
import jax
import jax.numpy as jnp
from jax import lax
from jax.sharding import PartitionSpec as P

epsilon = 1e-06


def steps_of(size):
    if size & (size - 1) == 0:
        return [(k, [(i, i ^ k) for i in range(size)]) for k in range(size - 1, 0, -1)]
    return [(k, [(i, (i + k) % size) for i in range(size)]) for k in range(1, size)]


def peer_of(rank, step, size):
    return rank ^ step if size & (size - 1) == 0 else (rank + step) % size


def source_of(rank, step, size):
    return rank ^ step if size & (size - 1) == 0 else (rank - step) % size


def reduce_over(chunks, axis, size, rank):
    total = lax.dynamic_index_in_dim(chunks, rank, 0, keepdims=False).astype(jnp.float32)
    for step, pairs in steps_of(size):
        sent = lax.dynamic_index_in_dim(chunks, peer_of(rank, step, size), 0, keepdims=False)
        total = total + lax.ppermute(sent, axis, pairs).astype(jnp.float32)
    return total


def gather_over(piece, axis, size, rank):
    whole = jnp.zeros((size,) + piece.shape, piece.dtype)
    whole = lax.dynamic_update_index_in_dim(whole, piece, rank, 0)
    for step, pairs in steps_of(size):
        got = lax.ppermute(piece, axis, pairs)
        whole = lax.dynamic_update_index_in_dim(whole, got, source_of(rank, step, size), 0)
    return whole


def project(scaled, weight):
    return jnp.dot(scaled, weight.reshape(weight.shape[0], -1), preferred_element_type=jnp.float32)


def scale_slab(slab_rows, gain_slice):
    rows_wide = slab_rows.astype(jnp.float32)
    return (
        (rows_wide * gain_slice.astype(jnp.float32)).astype(jnp.bfloat16),
        jnp.sum(rows_wide * rows_wide, axis=1),
    )


def cell_update(
    queries, keys_in, values_in, outgates, ingate, forget, memory, normalizer, stabilizer, head_scale
):
    head_dim = queries.shape[-1]
    query_wide = queries.astype(jnp.float32)
    key_scaled = keys_in.astype(jnp.float32) * head_dim ** (-0.5)
    value_wide = values_in.astype(jnp.float32)
    new_stabilizer = jnp.maximum(forget + stabilizer, ingate)
    retain = jnp.exp(forget + stabilizer - new_stabilizer)
    inflow = jnp.exp(ingate - new_stabilizer)
    new_memory = (
        retain[..., None, None] * memory
        + (inflow[..., None] * value_wide)[..., :, None] * key_scaled[..., None, :]
    )
    new_normalizer = retain[..., None] * normalizer + inflow[..., None] * key_scaled
    numerator = jnp.einsum("bhvk,bhk->bhv", new_memory, query_wide, precision=lax.Precision.HIGHEST)
    denominator = jnp.sum(new_normalizer * query_wide, axis=-1)
    readout = numerator / jnp.maximum(jnp.abs(denominator), jnp.exp(-new_stabilizer))[..., None]
    centered = readout - jnp.mean(readout, axis=-1, keepdims=True)
    normed = centered * lax.rsqrt(jnp.mean(centered * centered, axis=-1, keepdims=True) + epsilon)
    gated_out = (
        normed * head_scale.astype(jnp.float32) * jax.nn.sigmoid(outgates.astype(jnp.float32))
    )
    return (gated_out.astype(jnp.bfloat16), new_memory, new_normalizer, new_stabilizer)


def solution(mesh):
    n_kv = mesh.shape["kv"]
    n_tp = mesh.shape["tp"]

    def body(
        tokens,
        gain_mixer,
        weight_query,
        weight_key,
        weight_value,
        weight_outgate,
        weight_ingate,
        weight_forget,
        bias_input,
        bias_forget,
        memory,
        normalizer,
        stabilizer,
        head_gain,
        weight_out,
        gain_channel,
        weight_up,
        weight_down,
    ):
        kv_rank = lax.axis_index("kv")
        tp_rank = lax.axis_index("tp")
        own_rows, heads_here, head_dim = memory.shape[:3]
        rows, own_cols = tokens.shape
        width_full = gain_mixer.shape[0]
        wide = heads_here * head_dim
        head_start = tp_rank * heads_here
        slab_cols = own_cols * n_tp
        col_start = kv_rank * slab_cols
        slab = gather_over(tokens, "tp", n_tp, tp_rank)
        slab_rows = slab.transpose(1, 0, 2).reshape(rows, slab_cols)
        scaled, squares = scale_slab(
            slab_rows, lax.dynamic_slice_in_dim(gain_mixer, col_start, slab_cols, 0)
        )
        gate_weights = jnp.concatenate(
            [
                lax.dynamic_slice(weight_ingate, (col_start, head_start), (slab_cols, heads_here)),
                lax.dynamic_slice(weight_forget, (col_start, head_start), (slab_cols, heads_here)),
            ],
            axis=1,
        )
        gate_part = jnp.dot(scaled, gate_weights, preferred_element_type=jnp.float32)
        extra = jnp.concatenate(
            [gate_part, squares[:, None], jnp.zeros((rows, 127 - 2 * heads_here), jnp.float32)], axis=1
        )
        partials = [
            project(scaled, weight).astype(jnp.bfloat16)
            for weight in (weight_query, weight_key, weight_value, weight_outgate)
        ] + [extra.astype(jnp.bfloat16)]
        chunks = jnp.concatenate(partials, axis=1).reshape(n_kv, own_rows, -1)
        summed = reduce_over(chunks, "kv", n_kv, kv_rank)
        extra = summed[:, 4 * wide :]
        inverse = lax.rsqrt(extra[:, 2 * heads_here] / width_full + epsilon)[:, None]
        head_view = (own_rows, heads_here, head_dim)
        queries, keys_proj, values_proj, outgates = (
            (inverse * summed[:, j * wide : (j + 1) * wide]).astype(jnp.bfloat16).reshape(head_view)
            for j in range(4)
        )
        gate_pre = inverse * extra[:, : 2 * heads_here]
        ingate = gate_pre[:, :heads_here] + lax.dynamic_slice_in_dim(
            bias_input, head_start, heads_here, 0
        )
        forget = jax.nn.log_sigmoid(
            gate_pre[:, heads_here:]
            + lax.dynamic_slice_in_dim(bias_forget, head_start, heads_here, 0)
        )
        head_scale = lax.dynamic_slice_in_dim(head_gain, head_start, heads_here, 0)
        heads_out, new_memory, new_normalizer, new_stabilizer = cell_update(
            queries,
            keys_proj,
            values_proj,
            outgates,
            ingate,
            forget,
            memory,
            normalizer,
            stabilizer,
            head_scale,
        )
        heads_flat = gather_over(heads_out.reshape(own_rows, wide), "kv", n_kv, kv_rank)
        partial_out = jnp.dot(
            heads_flat.reshape(rows, wide), weight_out, preferred_element_type=jnp.float32
        ).astype(jnp.bfloat16)
        both = gather_over(partial_out, "tp", n_tp, tp_rank)
        mixed_slab = (
            slab_rows.astype(jnp.float32) + jnp.sum(both.astype(jnp.float32), axis=0)
        ).astype(jnp.bfloat16)
        mixed = gather_over(mixed_slab, "kv", n_kv, kv_rank)
        mixed_rows = mixed.transpose(1, 0, 2).reshape(rows, width_full)
        scaled_mlp, squares_mlp = scale_slab(mixed_rows, gain_channel)
        up_total = jnp.dot(scaled_mlp, weight_up, preferred_element_type=jnp.float32)
        inverse_mlp = lax.rsqrt(squares_mlp / width_full + epsilon)[:, None]
        activation = jax.nn.relu(inverse_mlp * up_total)
        squared = (activation * activation).astype(jnp.bfloat16)
        down = jnp.dot(squared, weight_down, preferred_element_type=jnp.float32)
        down = down.reshape(rows, n_kv, n_tp, own_cols).transpose(2, 1, 0, 3)
        here = reduce_over(down.astype(jnp.bfloat16), "tp", n_tp, tp_rank)
        here = reduce_over(here.astype(jnp.bfloat16), "kv", n_kv, kv_rank)
        mixed_own = lax.dynamic_slice_in_dim(mixed_slab, tp_rank * own_cols, own_cols, 1)
        layer_out = (mixed_own.astype(jnp.float32) + here).astype(jnp.bfloat16)
        return (layer_out, new_memory, new_normalizer, new_stabilizer)

    placed = (
        P("dp", ("kv", "tp")),
        P(),
        P("kv", "tp", None),
        P("kv", "tp", None),
        P("kv", "tp", None),
        P("kv", "tp", None),
        P(),
        P(),
        P(),
        P(),
        P(("dp", "kv"), "tp", None, None),
        P(("dp", "kv"), "tp", None),
        P(("dp", "kv"), "tp"),
        P(),
        P("tp", "kv"),
        P(),
        P(None, ("kv", "tp")),
        P(("kv", "tp"), None),
    )
    return jax.shard_map(
        body,
        mesh=mesh,
        in_specs=placed,
        out_specs=(
            P("dp", ("kv", "tp")),
            P(("dp", "kv"), "tp", None, None),
            P(("dp", "kv"), "tp", None),
            P(("dp", "kv"), "tp"),
        ),
        check_vma=False,
    )
```

time: 151 us -> 73.2 us (0.48)
  blocking collectives: 55.3 us -> 0 us
  waiting for transfers between devices: 39.4 us -> 17 us
  between operations: 15.7 us -> 1.13 us
  starting transfers between devices: 8.52 us -> 19.4 us
  local copies, waits for them, and re-layouts: 3.9 us -> 9.89 us
    reduce_scatter x2 -> x0, waiting for transfers between devices: 39.4 us -> none  [the longest x1 32.1 us: body(): lax.psum_scatter(jnp.einsum('uc,ru->cr', weight_block, squared, preferred...]
    all_gather x3 -> x0, blocking collectives: 29.8 us -> none  [the longest x1 14.3 us: body(): lax.all_gather(mixed_rows, ('kv', 'tp'), axis=1, tiled=True)]
    unnamed x2 -> x0, blocking collectives: 25.5 us -> none
    ppermute x0 -> x15, starting transfers between devices: none -> 19.4 us  [the longest x7 9.91 us: reduce_over(): total = total + lax.ppermute(sent, axis, pairs).astype(jnp.float32)]
    ppermute x0 -> x15, waiting for transfers between devices: none -> 17 us  [the longest x7 9.35 us: reduce_over(): total = total + lax.ppermute(sent, axis, pairs).astype(jnp.float32)]
    unnamed x4 -> x0, starting transfers between devices: 8.44 us -> none
    dynamic_update_slice x0 -> x11, local copies, waits for them, and re-layouts: none -> 4.29 us  [the longest x8 2.83 us: gather_over(): lax.dynamic_update_index_in_dim(whole, got, source_of(rank, step, size), 0)]
    convert_element_type x5 -> x9, other arithmetic: 3.09 us -> 1.65 us  [the longest x2 0.75 us: scale_slab(): gain_slice.astype(jnp.float32)]
  transfers between devices with their start and end apart: 6 -> 15, of which waited for: 2 -> 11; matrix products, arithmetic and copies ran while one was open for 1% -> 5% of each run, Pallas kernels for 0% -> 0%
where the time goes in v1:
time: 73.2 us; the launch traced here: 73 us
  starting transfers between devices  19.4 us (27%)
  matrix products  19.3 us (26%)
  waiting for transfers between devices  17 us (23%)
  local copies, waits for them, and re-layouts  9.89 us (14%)
  other arithmetic  6.31 us (9%)
  between operations  1.13 us (2%)
    dot_general x1, matrix products, body(): down = jnp.dot(squared, weight_down, preferred_element_type=jnp.float32)  12.9 us
    ppermute x7, starting transfers between devices, reduce_over(): total = total + lax.ppermute(sent, axis, pairs).astype(jnp.float32)  9.91 us
    ppermute x8, starting transfers between devices, gather_over(): got = lax.ppermute(piece, axis, pairs)  9.46 us
    ppermute x7, waiting for transfers between devices, reduce_over(): total = total + lax.ppermute(sent, axis, pairs).astype(jnp.float32)  9.35 us
    ppermute x8, waiting for transfers between devices, gather_over(): got = lax.ppermute(piece, axis, pairs)  7.68 us
    dot_general x4, matrix products, project(): jnp.dot(scaled, weight.reshape(weight.shape[0], -1), preferred_element_ty...  3.28 us
    unnamed x29, local copies, waits for them, and re-layouts  3.08 us
    dynamic_update_slice x8, local copies, waits for them, and re-layouts, gather_over(): lax.dynamic_update_index_in_dim(whole, got, source_of(rank, step, size), 0)  2.83 us
  transfers between devices with their start and end apart: 15, of which 11 were waited for; matrix products, arithmetic and copies ran while one was open for 5% of the time, Pallas kernels for 0%

profile of v1, /device:TPU:0, one launch (start us, length us, event | category | flops | bytes accessed | tf_op | source)
XLA Modules:
  0.0 73.0 jit_solution(17902728671305141632)
XLA Ops:
  1.2 0.7 %dynamic-slice_convert_fusion = f32[1024]{0:T(1024)S(1)} fusion(bf16[4096]{0:T(1024)(128)(2,1)} %param.19, s32[]{:T(128)} %select_n.63), kind=kLoop, calls=%fused_computation.105 | loop fusion | flops 1024 | bytes 6148 | tf_op jit(solution)/shard_map/convert_element_type | solution.py:47
  2.0 0.8 %copy.48 = bf16[1,24,512]{2,0,1:T(2,128)(2,1)S(1)} copy(bf16[1,24,512]{2,1,0:T(8,128)(2,1)} %bitcast.141) | data formatting | bytes 49152 | tf_op jit(solution)/shard_map/jit(dynamic_update_index_in_dim)/broadcast_in_dim | solution.py:33
  2.8 0.8 %dynamic_update_slice.40 = bf16[2,24,512]{2,0,1:T(2,128)(2,1)S(1)} dynamic-update-slice(bf16[2,24,512]{2,0,1:T(2,128)(2,1)S(1)} %broadcast_in_dim.73, bf16[1,24,512]{2,0,1:T(2,128)(2,1)S(1)} %copy.48, s32[]{:T(128)S(6)} %select_n.61, s32[]{:T(128)} %constant.99.clone.1, s32[]{:T(128)} %constant.99.clone.1) | dynamic-update-slice | bytes 49156 | tf_op jit(solution)/shard_map/jit(dynamic_update_index_in_dim)/dynamic_update_slice | solution.py:33
  3.6 0.8 %dynamic_update_slice.41 = bf16[2,24,512]{2,0,1:T(2,128)(2,1)S(1)} dynamic-update-slice(bf16[2,24,512]{2,0,1:T(2,128)(2,1)S(1)} %dynamic_update_slice.40, bf16[1,24,512]{2,0,1:T(2,128)(2,1)S(1)} %copy.49, s32[]{:T(128)S(6)} %select_n.62, s32[]{:T(128)} %constant.99.clone.1, s32[]{:T(128)} %constant.99.clone.1) | dynamic-update-slice | bytes 49156 | tf_op jit(solution)/shard_map/jit(dynamic_update_index_in_dim)/dynamic_update_slice | solution.py:36
  4.9 2.1 %fusion.24 = bf16[24,1024]{1,0:T(8,128)(2,1)S(1)} fusion(bf16[24,1024]{1,0:T(8,128)(2,1)S(1)} %bitcast.134, bf16[128,8,8,128]{3,2,1,0:T(8,128)(2,1)} %bitcast.147), kind=kOutput, calls=%fused_computation.21 | convolution fusion | flops 50356224 | bytes 2195456 | tf_op jit(solution)/shard_map/dot_general | solution.py:41
  8.1 0.7 copy-done.9
  9.7 4.7 %collective-permute-start.1 = (bf16[6,4224]{1,0:T(8,128)(2,1)S(1)}, bf16[6,4224]{1,0:T(8,128)(2,1)S(1)}, u32[]{:S(2)}, u32[]{:S(2)}) collective-permute-start(bf16[6,4224]{1,0:T(8,128)(2,1)S(1)} %get-tuple-element.9), channel_id=1, source_target_pairs={{0,6},{2,4},{4,2},{6,0},{1,7},{3,5},{5,3},{7,1},{8,14},{10,12},{12... | collective-permute-start | bytes 152072 | tf_op jit(solution)/shard_map/ppermute | solution.py:27
  14.5 0.6 collective-permute-start.2
  15.3 2.2 %collective-permute-done.1 = bf16[6,4224]{1,0:T(8,128)(2,1)S(1)} collective-permute-done((bf16[6,4224]{1,0:T(8,128)(2,1)S(1)}, bf16[6,4224]{1,0:T(8,128)(2,1)S(1)}, u32[]{:S(2)}, u32[]{:S(2)}) %collective-permute-start.1) | collective-permute-done | bytes 50720 | tf_op jit(solution)/shard_map/ppermute | solution.py:27
  17.5 2.4 %collective-permute-done.3 = bf16[6,4224]{1,0:T(8,128)(2,1)S(1)} collective-permute-done((bf16[6,4224]{1,0:T(8,128)(2,1)S(1)}, bf16[6,4224]{1,0:T(8,128)(2,1)S(1)}, u32[]{:S(2)}, u32[]{:S(2)}) %collective-permute-start.3) | collective-permute-done | bytes 50720 | tf_op jit(solution)/shard_map/ppermute | solution.py:27
  21.0 0.7 multiply_reduce_fusion.3
  21.7 2.5 %multiply_add_fusion = f32[6,8,128,128]{3,2,1,0:T(8,128)S(1)} fusion(f32[6,8,128,128]{3,2,1,0:T(8,128)} %param.28, f32[6,8,128]{2,1,0:T(8,128)S(1)} %get-tuple-element.25, f32[6,8,128]{2,1,0:T(8,128)S(1)} %get-tuple-element.28, f32[6,8]{1,0:T(8,128)S(1)} %subtract_exponential_fusion.1), kind=kLoop, calls=%fused_computation.1 | loop fusion | flops 2359296 | bytes 6340800 | tf_op jit(solution)/shard_map/add | solution.py:63
  24.2 1.7 %copy-done.1 = f32[6,8,128,128]{3,2,1,0:T(8,128)} copy-done((f32[6,8,128,128]{3,2,1,0:T(8,128)}, f32[6,8,128,128]{3,2,1,0:T(8,128)S(1)}, u32[]{:S(2)}) %copy-start.1) | copy-done | bytes 3145752
  25.9 2.5 %fusion.62 = f32[6,8,1,128]{3,2,1,0:T(1,128)S(1)} fusion(f32[6,8,128,128]{3,2,1,0:T(8,128)S(1)} %multiply_add_fusion, bf16[6,8,128,1]{2,3,1,0:T(2,128)(2,1)S(1)} %reshape.161), kind=kOutput, calls=%fused_computation.112 | convolution fusion | flops 9437184 | bytes 3182592 | tf_op jit(solution)/shard_map/bhvk,bhk->bhv/dot_general | solution.py:67
  28.9 1.4 %collective-permute-start.6 = (bf16[6,1024]{1,0:T(8,128)(2,1)S(1)}, bf16[6,1024]{1,0:T(8,128)(2,1)S(1)}, u32[]{:S(2)}, u32[]{:S(2)}) collective-permute-start(bf16[6,1024]{1,0:T(8,128)(2,1)S(1)} %bitcast.143), channel_id=1, source_target_pairs={{0,2},{2,0},{4,6},{6,4},{1,3},{3,1},{5,7},{7,5},{8,10},{10,8},{12,... | collective-permute-start | bytes 36872 | tf_op jit(solution)/shard_map/ppermute | solution.py:35
  30.3 1.6 %collective-permute-start.5 = (bf16[6,1024]{1,0:T(8,128)(2,1)S(1)}, bf16[6,1024]{1,0:T(8,128)(2,1)S(1)}, u32[]{:S(2)}, u32[]{:S(2)}) collective-permute-start(bf16[6,1024]{1,0:T(8,128)(2,1)S(1)} %bitcast.144), channel_id=1, source_target_pairs={{0,4},{2,6},{4,0},{6,2},{1,5},{3,7},{5,1},{7,3},{8,12},{10,14},{12... | collective-permute-start | bytes 36872 | tf_op jit(solution)/shard_map/ppermute | solution.py:35
  31.9 1.5 %collective-permute-start.4 = (bf16[6,1024]{1,0:T(8,128)(2,1)S(1)}, bf16[6,1024]{1,0:T(8,128)(2,1)S(1)}, u32[]{:S(2)}, u32[]{:S(2)}) collective-permute-start(bf16[6,1024]{1,0:T(8,128)(2,1)S(1)} %bitcast.145), channel_id=1, source_target_pairs={{0,6},{2,4},{4,2},{6,0},{1,7},{3,5},{5,3},{7,1},{8,14},{10,12},{12... | collective-permute-start | bytes 36872 | tf_op jit(solution)/shard_map/ppermute | solution.py:35
  33.4 4.0 %collective-permute-done.4 = bf16[6,1024]{1,0:T(8,128)(2,1)S(1)} collective-permute-done((bf16[6,1024]{1,0:T(8,128)(2,1)S(1)}, bf16[6,1024]{1,0:T(8,128)(2,1)S(1)}, u32[]{:S(2)}, u32[]{:S(2)}) %collective-permute-start.4) | collective-permute-done | bytes 12320 | tf_op jit(solution)/shard_map/ppermute | solution.py:35
  38.1 1.1 %collective-permute-done.7 = bf16[24,1024]{1,0:T(8,128)(2,1)S(1)} collective-permute-done((bf16[24,1024]{1,0:T(8,128)(2,1)S(1)}, bf16[24,1024]{1,0:T(8,128)(2,1)S(1)}, u32[]{:S(2)}, u32[]{:S(2)}) %collective-permute-start.7) | collective-permute-done | bytes 49184 | tf_op jit(solution)/shard_map/ppermute | solution.py:35
  39.3 2.0 %collective-permute-start.9 = (bf16[24,1024]{1,0:T(8,128)(2,1)S(1)}, bf16[24,1024]{1,0:T(8,128)(2,1)S(1)}, u32[]{:S(2)}, u32[]{:S(2)}) collective-permute-start(bf16[24,1024]{1,0:T(8,128)(2,1)S(1)} %add_convert_fusion), channel_id=1, source_target_pairs={{0,4},{2,6},{4,0},{6,2},{1,5},{3,7},{5,1},{7,3},{8,12},{10,14},{12... | collective-permute-start | bytes 147464 | tf_op jit(solution)/shard_map/ppermute | solution.py:35
  41.3 2.3 %collective-permute-start.8 = (bf16[24,1024]{1,0:T(8,128)(2,1)S(1)}, bf16[24,1024]{1,0:T(8,128)(2,1)S(1)}, u32[]{:S(2)}, u32[]{:S(2)}) collective-permute-start(bf16[24,1024]{1,0:T(8,128)(2,1)S(1)} %add_convert_fusion), channel_id=1, source_target_pairs={{0,6},{2,4},{4,2},{6,0},{1,7},{3,5},{5,3},{7,1},{8,14},{10,12},{12... | collective-permute-start | bytes 147464 | tf_op jit(solution)/shard_map/ppermute | solution.py:35
  43.9 0.7 dynamic_update_slice.48
  45.2 2.0 %collective-permute-done.8 = bf16[24,1024]{1,0:T(8,128)(2,1)S(1)} collective-permute-done((bf16[24,1024]{1,0:T(8,128)(2,1)S(1)}, bf16[24,1024]{1,0:T(8,128)(2,1)S(1)}, u32[]{:S(2)}, u32[]{:S(2)}) %collective-permute-start.8) | collective-permute-done | bytes 49184 | tf_op jit(solution)/shard_map/ppermute | solution.py:35
  47.3 0.7 dynamic_update_slice.49
  48.0 0.7 dynamic_update_slice.50
  48.7 0.7 dynamic_update_slice.51
  49.9 12.9 %convolution_convert_fusion = bf16[24,4096]{1,0:T(8,128)(2,1)S(1)} fusion(bf16[2048,4096]{1,0:T(8,128)(2,1)} %param.35, bf16[4096,2048]{1,0:T(8,128)(2,1)} %param.34, f32[24,4096]{1,0:T(8,128)S(1)} %bitcast.122, f32[4096]{0:T(1024)S(1)} %convert_element_type.245, f32[24]{0:T(128)S(1)} %add_rsqrt_fusion.1), kind=kOutput, calls=%fused_computation | convolution fusion | flops 805797888 | bytes 34160736 | tf_op jit(solution)/shard_map/dot_general | solution.py:176
  63.6 1.3 %collective-permute-done.11 = bf16[4,24,512]{2,1,0:T(8,128)(2,1)S(1)} collective-permute-done((bf16[4,24,512]{2,1,0:T(8,128)(2,1)S(1)}, bf16[4,24,512]{2,1,0:T(8,128)(2,1)S(1)}, u32[]{:S(2)}, u32[]{:S(2)}) %collective-permute-start.11) | collective-permute-done | bytes 98336 | tf_op jit(solution)/shard_map/ppermute | solution.py:27
  65.0 2.4 %collective-permute-start.12 = (bf16[24,512]{1,0:T(8,128)(2,1)S(1)}, bf16[24,512]{1,0:T(8,128)(2,1)S(1)}, u32[]{:S(2)}, u32[]{:S(2)}) collective-permute-start(bf16[24,512]{1,0:T(8,128)(2,1)S(1)} %get-tuple-element.18), channel_id=1, source_target_pairs={{0,6},{2,4},{4,2},{6,0},{1,7},{3,5},{5,3},{7,1},{8,14},{10,12},{12... | collective-permute-start | bytes 73736 | tf_op jit(solution)/shard_map/ppermute | solution.py:27
  67.4 2.0 %collective-permute-start.13 = (bf16[24,512]{1,0:T(8,128)(2,1)S(1)}, bf16[24,512]{1,0:T(8,128)(2,1)S(1)}, u32[]{:S(2)}, u32[]{:S(2)}) collective-permute-start(bf16[24,512]{1,0:T(8,128)(2,1)S(1)} %get-tuple-element.20), channel_id=1, source_target_pairs={{0,4},{2,6},{4,0},{6,2},{1,5},{3,7},{5,1},{7,3},{8,12},{10,14},{12... | collective-permute-start | bytes 73736 | tf_op jit(solution)/shard_map/ppermute | solution.py:27
  69.4 1.2 %collective-permute-done.12 = bf16[24,512]{1,0:T(8,128)(2,1)S(1)} collective-permute-done((bf16[24,512]{1,0:T(8,128)(2,1)S(1)}, bf16[24,512]{1,0:T(8,128)(2,1)S(1)}, u32[]{:S(2)}, u32[]{:S(2)}) %collective-permute-start.12) | collective-permute-done | bytes 24608 | tf_op jit(solution)/shard_map/ppermute | solution.py:27
  71.3 1.1 %collective-permute-done.13 = bf16[24,512]{1,0:T(8,128)(2,1)S(1)} collective-permute-done((bf16[24,512]{1,0:T(8,128)(2,1)S(1)}, bf16[24,512]{1,0:T(8,128)(2,1)S(1)}, u32[]{:S(2)}, u32[]{:S(2)}) %collective-permute-start.13) | collective-permute-done | bytes 24608 | tf_op jit(solution)/shard_map/ppermute | solution.py:27
  (103 shorter events, 8.9 us)
Async XLA Ops:
  0.6 36.9 %copy-start = (bf16[1024,1024]{1,0:T(8,128)(2,1)S(1)}, bf16[1024,1024]{1,0:T(8,128)(2,1)}, u32[]{:S(2)}) copy-start(bf16[1024,1024]{1,0:T(8,128)(2,1)} %param.32) | copy-start | bytes 6291460
  0.6 2.9 %collective-permute-start = (bf16[24,512]{1,0:T(8,128)(2,1)}, bf16[24,512]{1,0:T(8,128)(2,1)S(1)}, u32[]{:S(2)}, u32[]{:S(2)}) collective-permute-start(bf16[24,512]{1,0:T(8,128)(2,1)} %param.18), channel_id=1, source_target_pairs={{0,1},{1,0},{2,3},{3,2},{4,5},{5,4},{6,7},{7,6},{8,9},{9,8},{10,11... | collective-permute-start | bytes 73736 | tf_op jit(solution)/shard_map/ppermute | solution.py:35
  4.9 2.2 %copy-start.7 = (bf16[1024,8,128]{2,1,0:T(8,128)(2,1)S(1)}, bf16[1024,8,128]{2,1,0:T(8,128)(2,1)}, u32[]{:S(2)}) copy-start(bf16[1024,8,128]{2,1,0:T(8,128)(2,1)} %param.22) | copy-start | bytes 6291460
  4.9 2.9 %copy-start.8 = (bf16[1024,8,128]{2,1,0:T(8,128)(2,1)S(1)}, bf16[1024,8,128]{2,1,0:T(8,128)(2,1)}, u32[]{:S(2)}) copy-start(bf16[1024,8,128]{2,1,0:T(8,128)(2,1)} %param.21) | copy-start | bytes 6291460
  7.1 1.7 %copy-start.9 = (bf16[1024,8,128]{2,1,0:T(8,128)(2,1)S(1)}, bf16[1024,8,128]{2,1,0:T(8,128)(2,1)}, u32[]{:S(2)}) copy-start(bf16[1024,8,128]{2,1,0:T(8,128)(2,1)} %param.20) | copy-start | bytes 6291460
  7.7 1.5 %dynamic-slice-start = ((bf16[4096,16]{0,1:T(8,128)(2,1)}, s32[]{:T(128)}, s32[]{:T(128)}), bf16[1024,8]{0,1:T(8,128)(2,1)S(1)}, s32[]{:S(2)}) async-start(bf16[4096,16]{0,1:T(8,128)(2,1)} %param.24, s32[]{:T(128)} %select_n.63, s32[]{:T(128)} %select_n.64), calls=%async_computation | async-start | bytes 33280 | tf_op jit(solution)/shard_map/dynamic_slice | solution.py:118
  7.7 1.5 %dynamic-slice-start.1 = ((bf16[4096,16]{0,1:T(8,128)(2,1)}, s32[]{:T(128)}, s32[]{:T(128)}), bf16[1024,8]{0,1:T(8,128)(2,1)S(1)}, s32[]{:S(2)}) async-start(bf16[4096,16]{0,1:T(8,128)(2,1)} %param.25, s32[]{:T(128)} %select_n.63, s32[]{:T(128)} %select_n.64), calls=%async_computation.1 | async-start | bytes 33280 | tf_op jit(solution)/shard_map/dynamic_slice | solution.py:119
  8.1 7.0 %copy-start.6 = (bf16[16,128]{1,0:T(8,128)(2,1)S(1)}, bf16[16,128]{1,0:T(8,128)(2,1)}, u32[]{:S(2)}) copy-start(bf16[16,128]{1,0:T(8,128)(2,1)} %param.31) | copy-start | bytes 12292
  8.1 7.0 %copy-start.10 = (f32[16]{0:T(128)S(1)}, f32[16]{0:T(128)}, u32[]{:S(2)}) copy-start(f32[16]{0:T(128)} %param.27) | copy-start | bytes 196
  8.1 7.1 %copy-start.11 = (f32[16]{0:T(128)S(1)}, f32[16]{0:T(128)}, u32[]{:S(2)}) copy-start(f32[16]{0:T(128)} %param.26) | copy-start | bytes 196
  8.8 12.0 %copy-start.4 = (f32[6,8]{1,0:T(8,128)S(1)}, f32[6,8]{1,0:T(8,128)}, u32[]{:S(2)}) copy-start(f32[6,8]{1,0:T(8,128)} %param.30) | copy-start | bytes 580
  8.8 12.2 %copy-start.3 = (f32[6,8,128]{2,1,0:T(8,128)S(1)}, f32[6,8,128]{2,1,0:T(8,128)}, u32[]{:S(2)}) copy-start(f32[6,8,128]{2,1,0:T(8,128)} %param.29) | copy-start | bytes 73732
  9.7 7.8 %collective-permute-start.1 = (bf16[6,4224]{1,0:T(8,128)(2,1)S(1)}, bf16[6,4224]{1,0:T(8,128)(2,1)S(1)}, u32[]{:S(2)}, u32[]{:S(2)}) collective-permute-start(bf16[6,4224]{1,0:T(8,128)(2,1)S(1)} %get-tuple-element.9), channel_id=1, source_target_pairs={{0,6},{2,4},{4,2},{6,0},{1,7},{3,5},{5,3},{7,1},{8,14},{10,12},{12... | collective-permute-start | bytes 152072 | tf_op jit(solution)/shard_map/ppermute | solution.py:27
  14.5 5.4 %collective-permute-start.3 = (bf16[6,4224]{1,0:T(8,128)(2,1)S(1)}, bf16[6,4224]{1,0:T(8,128)(2,1)S(1)}, u32[]{:S(2)}, u32[]{:S(2)}) collective-permute-start(bf16[6,4224]{1,0:T(8,128)(2,1)S(1)} %get-tuple-element.10), channel_id=1, source_target_pairs={{0,2},{2,0},{4,6},{6,4},{1,3},{3,1},{5,7},{7,5},{8,10},{10,8},{12,... | collective-permute-start | bytes 152072 | tf_op jit(solution)/shard_map/ppermute | solution.py:27
  14.5 5.9 %collective-permute-start.2 = (bf16[6,4224]{1,0:T(8,128)(2,1)S(1)}, bf16[6,4224]{1,0:T(8,128)(2,1)S(1)}, u32[]{:S(2)}, u32[]{:S(2)}) collective-permute-start(bf16[6,4224]{1,0:T(8,128)(2,1)S(1)} %get-tuple-element.11), channel_id=1, source_target_pairs={{0,4},{2,6},{4,0},{6,2},{1,5},{3,7},{5,1},{7,3},{8,12},{10,14},{12... | collective-permute-start | bytes 152072 | tf_op jit(solution)/shard_map/ppermute | solution.py:27
  20.9 3.3 %copy-start.2 = (f32[6,8]{1,0:T(8,128)}, f32[6,8]{1,0:T(8,128)S(1)}, u32[]{:S(2)}) copy-start(f32[6,8]{1,0:T(8,128)S(1)} %get-tuple-element.8) | copy-start | bytes 580
  24.2 1.7 %copy-start.1 = (f32[6,8,128,128]{3,2,1,0:T(8,128)}, f32[6,8,128,128]{3,2,1,0:T(8,128)S(1)}, u32[]{:S(2)}) copy-start(f32[6,8,128,128]{3,2,1,0:T(8,128)S(1)} %multiply_add_fusion) | copy-start | bytes 9437188
  28.4 9.5 %copy-start.5 = (bf16[4096]{0:T(1024)(128)(2,1)S(1)}, bf16[4096]{0:T(1024)(128)(2,1)}, u32[]{:S(2)}) copy-start(bf16[4096]{0:T(1024)(128)(2,1)} %param.33) | copy-start | bytes 24580
  28.9 8.5 %collective-permute-start.6 = (bf16[6,1024]{1,0:T(8,128)(2,1)S(1)}, bf16[6,1024]{1,0:T(8,128)(2,1)S(1)}, u32[]{:S(2)}, u32[]{:S(2)}) collective-permute-start(bf16[6,1024]{1,0:T(8,128)(2,1)S(1)} %bitcast.143), channel_id=1, source_target_pairs={{0,2},{2,0},{4,6},{6,4},{1,3},{3,1},{5,7},{7,5},{8,10},{10,8},{12,... | collective-permute-start | bytes 36872 | tf_op jit(solution)/shard_map/ppermute | solution.py:35
  30.3 7.2 %collective-permute-start.5 = (bf16[6,1024]{1,0:T(8,128)(2,1)S(1)}, bf16[6,1024]{1,0:T(8,128)(2,1)S(1)}, u32[]{:S(2)}, u32[]{:S(2)}) collective-permute-start(bf16[6,1024]{1,0:T(8,128)(2,1)S(1)} %bitcast.144), channel_id=1, source_target_pairs={{0,4},{2,6},{4,0},{6,2},{1,5},{3,7},{5,1},{7,3},{8,12},{10,14},{12... | collective-permute-start | bytes 36872 | tf_op jit(solution)/shard_map/ppermute | solution.py:35
  31.9 5.5 %collective-permute-start.4 = (bf16[6,1024]{1,0:T(8,128)(2,1)S(1)}, bf16[6,1024]{1,0:T(8,128)(2,1)S(1)}, u32[]{:S(2)}, u32[]{:S(2)}) collective-permute-start(bf16[6,1024]{1,0:T(8,128)(2,1)S(1)} %bitcast.145), channel_id=1, source_target_pairs={{0,6},{2,4},{4,2},{6,0},{1,7},{3,5},{5,3},{7,1},{8,14},{10,12},{12... | collective-permute-start | bytes 36872 | tf_op jit(solution)/shard_map/ppermute | solution.py:35
  38.0 1.2 %collective-permute-start.7 = (bf16[24,1024]{1,0:T(8,128)(2,1)S(1)}, bf16[24,1024]{1,0:T(8,128)(2,1)S(1)}, u32[]{:S(2)}, u32[]{:S(2)}) collective-permute-start(bf16[24,1024]{1,0:T(8,128)(2,1)S(1)} %get-tuple-element.27), channel_id=1, source_target_pairs={{0,1},{1,0},{2,3},{3,2},{4,5},{5,4},{6,7},{7,6},{8,9},{9,8},{10,11... | collective-permute-start | bytes 147464 | tf_op jit(solution)/shard_map/ppermute | solution.py:35
  39.2 5.3 %collective-permute-start.10 = (bf16[24,1024]{1,0:T(8,128)(2,1)S(1)}, bf16[24,1024]{1,0:T(8,128)(2,1)S(1)}, u32[]{:S(2)}, u32[]{:S(2)}) collective-permute-start(bf16[24,1024]{1,0:T(8,128)(2,1)S(1)} %add_convert_fusion), channel_id=1, source_target_pairs={{0,2},{2,0},{4,6},{6,4},{1,3},{3,1},{5,7},{7,5},{8,10},{10,8},{12,... | collective-permute-start | bytes 147464 | tf_op jit(solution)/shard_map/ppermute | solution.py:35
  39.3 5.8 %collective-permute-start.9 = (bf16[24,1024]{1,0:T(8,128)(2,1)S(1)}, bf16[24,1024]{1,0:T(8,128)(2,1)S(1)}, u32[]{:S(2)}, u32[]{:S(2)}) collective-permute-start(bf16[24,1024]{1,0:T(8,128)(2,1)S(1)} %add_convert_fusion), channel_id=1, source_target_pairs={{0,4},{2,6},{4,0},{6,2},{1,5},{3,7},{5,1},{7,3},{8,12},{10,14},{12... | collective-permute-start | bytes 147464 | tf_op jit(solution)/shard_map/ppermute | solution.py:35
  41.3 5.9 %collective-permute-start.8 = (bf16[24,1024]{1,0:T(8,128)(2,1)S(1)}, bf16[24,1024]{1,0:T(8,128)(2,1)S(1)}, u32[]{:S(2)}, u32[]{:S(2)}) collective-permute-start(bf16[24,1024]{1,0:T(8,128)(2,1)S(1)} %add_convert_fusion), channel_id=1, source_target_pairs={{0,6},{2,4},{4,2},{6,0},{1,7},{3,5},{5,3},{7,1},{8,14},{10,12},{12... | collective-permute-start | bytes 147464 | tf_op jit(solution)/shard_map/ppermute | solution.py:35
  63.5 1.4 %collective-permute-start.11 = (bf16[4,24,512]{2,1,0:T(8,128)(2,1)S(1)}, bf16[4,24,512]{2,1,0:T(8,128)(2,1)S(1)}, u32[]{:S(2)}, u32[]{:S(2)}) collective-permute-start(bf16[4,24,512]{2,1,0:T(8,128)(2,1)S(1)} %bitcast.133), channel_id=1, source_target_pairs={{0,1},{1,0},{2,3},{3,2},{4,5},{5,4},{6,7},{7,6},{8,9},{9,8},{10,11... | collective-permute-start | bytes 294920 | tf_op jit(solution)/shard_map/ppermute | solution.py:27
  65.0 5.7 %collective-permute-start.12 = (bf16[24,512]{1,0:T(8,128)(2,1)S(1)}, bf16[24,512]{1,0:T(8,128)(2,1)S(1)}, u32[]{:S(2)}, u32[]{:S(2)}) collective-permute-start(bf16[24,512]{1,0:T(8,128)(2,1)S(1)} %get-tuple-element.18), channel_id=1, source_target_pairs={{0,6},{2,4},{4,2},{6,0},{1,7},{3,5},{5,3},{7,1},{8,14},{10,12},{12... | collective-permute-start | bytes 73736 | tf_op jit(solution)/shard_map/ppermute | solution.py:27
  67.4 3.9 %collective-permute-start.14 = (bf16[24,512]{1,0:T(8,128)(2,1)S(1)}, bf16[24,512]{1,0:T(8,128)(2,1)S(1)}, u32[]{:S(2)}, u32[]{:S(2)}) collective-permute-start(bf16[24,512]{1,0:T(8,128)(2,1)S(1)} %get-tuple-element.19), channel_id=1, source_target_pairs={{0,2},{2,0},{4,6},{6,4},{1,3},{3,1},{5,7},{7,5},{8,10},{10,8},{12,... | collective-permute-start | bytes 73736 | tf_op jit(solution)/shard_map/ppermute | solution.py:27
  67.4 5.0 %collective-permute-start.13 = (bf16[24,512]{1,0:T(8,128)(2,1)S(1)}, bf16[24,512]{1,0:T(8,128)(2,1)S(1)}, u32[]{:S(2)}, u32[]{:S(2)}) collective-permute-start(bf16[24,512]{1,0:T(8,128)(2,1)S(1)} %get-tuple-element.20), channel_id=1, source_target_pairs={{0,4},{2,6},{4,0},{6,2},{1,5},{3,7},{5,1},{7,3},{8,12},{10,14},{12... | collective-permute-start | bytes 73736 | tf_op jit(solution)/shard_map/ppermute | solution.py:27

commit v2 on v1

--- a/solution.py
+++ b/solution.py
@@ -1,6 +1,8 @@
 import jax
 import jax.numpy as jnp
 from jax import lax
+from jax.experimental import pallas as pl
+from jax.experimental.pallas import tpu as pltpu
 from jax.sharding import PartitionSpec as P
 
 epsilon = 1e-06
@@ -73,6 +75,332 @@
         normed * head_scale.astype(jnp.float32) * jax.nn.sigmoid(outgates.astype(jnp.float32))
     )
     return (gated_out.astype(jnp.bfloat16), new_memory, new_normalizer, new_stabilizer)
+
+
+MIB = 1024 * 1024
+VMEM = pl.BlockSpec(memory_space=pltpu.VMEM)
+SMEM = pl.BlockSpec(memory_space=pltpu.SMEM)
+WIDE = jnp.float32
+NARROW = jnp.bfloat16
+
+
+def shaped(shape, dtype):
+    return jax.ShapeDtypeStruct(shape, dtype)
+
+
+def kernel_call(ranks, kernel, name, outs, args, scratch=(), limit=8, cost_us=0, specs=None):
+    single = not isinstance(outs, (list, tuple))
+    cost = pl.CostEstimate(
+        flops=int(cost_us * 1e9) + 1, bytes_accessed=int(cost_us * 3e6) + 1, transcendentals=0
+    )
+    return pl.pallas_call(
+        kernel,
+        out_shape=outs if single else tuple(outs),
+        in_specs=[SMEM, SMEM] + (specs or [VMEM] * len(args)),
+        out_specs=VMEM if single else (VMEM,) * len(outs),
+        scratch_shapes=scratch,
+        compiler_params=pltpu.CompilerParams(vmem_limit_bytes=limit * MIB),
+        cost_estimate=cost,
+        name=name,
+    )(*ranks, *args)
+
+
+def load_first(ranks, tokens, gain_tiles, in_rows, forget_rows, weights, heads_here, cols):
+    parts = cols // 128
+    count = 4 + len(weights)
+
+    def kernel(kv_ref, tp_ref, tokens_ref, gain_ref, in_ref, forget_ref, *refs):
+        weight_refs, outs, sems = refs[: len(weights)], refs[len(weights) : -1], refs[-1]
+        mine_ref, own_gain_ref, gates_ref = outs[:3]
+        tile = pl.multiple_of(kv_ref[0] * parts, 8)
+        start = pl.multiple_of(kv_ref[0] * cols, 128)
+        head = pl.multiple_of(tp_ref[0] * heads_here, 8)
+        window = (pl.ds(head, heads_here), pl.ds(start, cols))
+        pairs = [
+            (tokens_ref, mine_ref),
+            (gain_ref.at[pl.ds(tile, parts), :], own_gain_ref),
+            (in_ref.at[window], gates_ref.at[pl.ds(0, heads_here), :]),
+            (forget_ref.at[window], gates_ref.at[pl.ds(heads_here, heads_here), :]),
+            *zip(weight_refs, outs[3:]),
+        ]
+        copies = [pltpu.make_async_copy(*pair, sems.at[n]) for n, pair in enumerate(pairs)]
+        for copy in copies:
+            copy.start()
+        for copy in copies:
+            copy.wait()
+
+    args = (tokens, gain_tiles, in_rows, forget_rows, *weights)
+    return kernel_call(
+        ranks,
+        kernel,
+        "load_first",
+        [
+            shaped(tokens.shape, NARROW),
+            shaped((parts, 128), NARROW),
+            shaped((2 * heads_here, cols), NARROW),
+        ]
+        + [pltpu.VMEM(weight.shape, NARROW) for weight in weights],
+        [pltpu.with_memory_space_constraint(arg, pltpu.HBM) for arg in args],
+        scratch=[pltpu.SemaphoreType.DMA((count,))],
+        cost_us=COST_LOAD,
+        specs=[pl.BlockSpec(memory_space=pl.ANY)] * count,
+    )
+
+
+def start_block(ranks, mine, other, own_gain, gates):
+    rows, own_cols = mine.shape
+    cols = 2 * own_cols
+    count = gates.shape[0]
+
+    def kernel(kv_ref, tp_ref, mine_ref, other_ref, gain_ref, gates_ref, slab_ref, scaled_ref, extra_ref):
+        first = tp_ref[0] == 0
+        own = mine_ref[...].astype(WIDE)
+        theirs = other_ref[...].astype(WIDE)
+        gain = gain_ref[...].astype(WIDE)
+        halves = (jnp.where(first, own, theirs), jnp.where(first, theirs, own))
+        squares = jnp.zeros((rows, 1), WIDE)
+        for half, slab in enumerate(halves):
+            squares = squares + jnp.sum(slab * slab, axis=1, keepdims=True)
+            slab_ref[:, half * own_cols : (half + 1) * own_cols] = slab.astype(NARROW)
+            for part in range(own_cols // 128):
+                tile = half * (own_cols // 128) + part
+                scaled_ref[:, tile * 128 : (tile + 1) * 128] = (
+                    slab[:, part * 128 : (part + 1) * 128] * gain[tile : tile + 1, :]
+                ).astype(NARROW)
+        extra_ref[...] = jnp.zeros(extra_ref.shape, WIDE)
+        extra_ref[:, :count] = lax.dot_general(
+            scaled_ref[...], gates_ref[...], (((1,), (1,)), ((), ())), preferred_element_type=WIDE
+        )
+        extra_ref[:, count : count + 1] = squares
+
+    return kernel_call(
+        ranks,
+        kernel,
+        "start_block",
+        [shaped((rows, cols), NARROW), shaped((rows, cols), NARROW), shaped((rows, 128), WIDE)],
+        (mine, other, own_gain, gates),
+    )
+
+
+def pack(ranks, partials, extra, n_kv):
+    rows, wide = partials[0].shape
+    own = rows // n_kv
+    kinds = len(partials)
+    steps = [step for step, _ in steps_of(n_kv)]
+    shape = (kinds * own, wide + 128)
+
+    def kernel(kv_ref, tp_ref, *refs):
+        parts, extra_ref, outs, scratch = refs[:kinds], refs[kinds], refs[kinds + 1 : -1], refs[-1]
+        scratch[:, :, wide:] = jnp.zeros((n_kv, kinds * own, 128), WIDE)
+        for j in range(n_kv):
+            for m in range(kinds):
+                scratch[j, m * own : (m + 1) * own, :wide] = parts[m][j * own : (j + 1) * own, :]
+            scratch[j, :own, wide:] = extra_ref[j * own : (j + 1) * own, :]
+        outs[0][...] = scratch[kv_ref[0]]
+        for out, step in zip(outs[1:], steps):
+            out[...] = scratch[kv_ref[0] ^ step].astype(NARROW)
+
+    return kernel_call(
+        ranks,
+        kernel,
+        "pack",
+        [shaped(shape, WIDE)] + [shaped(shape, NARROW)] * len(steps),
+        (*partials, extra),
+        scratch=[pltpu.VMEM((n_kv,) + shape, WIDE)],
+        cost_us=COST_PACK,
+    )
+
+
+def cell(ranks, parts, bias_in, bias_forget, stabilizer, normalizer, head_gain, memory, width_full):
+    own, heads, dim = normalizer.shape
+    wide = heads * dim
+    count = len(parts)
+
+    def kernel(kv_ref, tp_ref, *refs):
+        part_refs = refs[:count]
+        (bias_in_ref, bias_forget_ref, stab_ref, norm_ref, gain_ref, memory_ref) = refs[count : count + 6]
+        (heads_ref, new_norm_ref, new_stab_ref, retain_ref, values_ref, keys_ref, scratch) = refs[count + 6 :]
+        total = part_refs[0][...]
+        for ref in part_refs[1:]:
+            total = total + ref[...].astype(WIDE)
+        scratch[...] = total
+        tp = tp_ref[0]
+        inverse = lax.rsqrt(
+            scratch[0:own, wide + 2 * heads : wide + 2 * heads + 1] / width_full + epsilon
+        )
+
+        def bias(ref):
+            return jnp.where(tp == 0, ref[:, 0:heads], ref[:, heads : 2 * heads])
+
+        ingate = inverse * scratch[0:own, wide : wide + heads] + bias(bias_in_ref)
+        pre = inverse * scratch[0:own, wide + heads : wide + 2 * heads] + bias(bias_forget_ref)
+        forget = jnp.minimum(pre, 0.0) - jnp.log1p(jnp.exp(-jnp.abs(pre)))
+        carried = forget + stab_ref[...]
+        new_stab = jnp.maximum(carried, ingate)
+        retain = jnp.exp(carried - new_stab)
+        inflow = jnp.exp(ingate - new_stab)
+        floor = jnp.exp(-new_stab)
+        new_stab_ref[...] = new_stab
+        retain_ref[...] = retain
+        gains = gain_ref[pl.ds(pl.multiple_of(tp * heads, 8), heads), :].astype(WIDE)
+        which = lax.broadcasted_iota(jnp.int32, (own, dim), 0)
+        for h in range(heads):
+            lanes = slice(h * dim, (h + 1) * dim)
+            query, key, value, gate = (
+                (inverse * scratch[m * own : (m + 1) * own, lanes]).astype(NARROW) for m in range(4)
+            )
+            query_wide = query.astype(WIDE)
+            key_scaled = key.astype(WIDE) * dim ** (-0.5)
+            keep = retain[:, h : h + 1]
+            value_in = inflow[:, h : h + 1] * value.astype(WIDE)
+            keys_ref[:, h, :] = key_scaled
+            values_ref[:, h, :] = value_in
+            new_norm = keep * norm_ref[:, h, :] + inflow[:, h : h + 1] * key_scaled
+            new_norm_ref[:, h, :] = new_norm
+            denominator = jnp.sum(new_norm * query_wide, axis=1, keepdims=True)
+            overlap = jnp.sum(key_scaled * query_wide, axis=1, keepdims=True)
+            held = jnp.zeros((own, dim), WIDE)
+            for b in range(own):
+                block = memory_ref[b, h]
+                high = block.astype(NARROW)
+                low = (block - high.astype(WIDE)).astype(NARROW)
+                dims = (((1,), (1,)), ((), ()))
+                got = lax.dot_general(query, high, dims, preferred_element_type=WIDE)
+                got = got + lax.dot_general(query, low, dims, preferred_element_type=WIDE)
+                held = jnp.where(which == b, got, held)
+            numerator = keep * held + value_in * overlap
+            readout = numerator / jnp.maximum(jnp.abs(denominator), floor[:, h : h + 1])
+            centered = readout - jnp.mean(readout, axis=1, keepdims=True)
+            normed = centered * lax.rsqrt(jnp.mean(centered * centered, axis=1, keepdims=True) + epsilon)
+            gated = normed * gains[h : h + 1, :] / (1.0 + jnp.exp(-gate.astype(WIDE)))
+            heads_ref[:, lanes] = gated.astype(NARROW)
+
+    return kernel_call(
+        ranks,
+        kernel,
+        "cell",
+        [
+            shaped((own, wide), NARROW),
+            shaped(normalizer.shape, WIDE),
+            shaped(stabilizer.shape, WIDE),
+            shaped(stabilizer.shape, WIDE),
+            shaped(normalizer.shape, WIDE),
+            shaped(normalizer.shape, WIDE),
+        ],
+        (*parts, bias_in, bias_forget, stabilizer, normalizer, head_gain, memory),
+        scratch=[pltpu.VMEM(parts[0].shape, WIDE)],
+        cost_us=COST_CELL,
+    )
+
+
+def out_step(ranks, own_heads, arrived, weight_out, later, n_kv):
+    own, wide = own_heads.shape
+    rows = own * n_kv
+    steps = [step for step, _ in steps_of(n_kv)]
+
+    def kernel(kv_ref, tp_ref, own_ref, *refs):
+        got, weight_ref = refs[: len(steps)], refs[len(steps)]
+        out_ref, stacked, flat = refs[-3:]
+        kv = kv_ref[0]
+        stacked[kv, :own, :] = own_ref[...].astype(WIDE)
+        for ref, step in zip(got, steps):
+            stacked[kv ^ step, :own, :] = ref[...].astype(WIDE)
+        for j in range(n_kv):
+            flat[j * own : (j + 1) * own, :] = stacked[j, :own, :]
+        out_ref[...] = jnp.dot(
+            flat[...].astype(NARROW), weight_ref[...], preferred_element_type=WIDE
+        ).astype(NARROW)
+
+    return kernel_call(
+        ranks,
+        kernel,
+        "out_step",
+        shaped((rows, weight_out.shape[1]), NARROW),
+        (own_heads, *arrived, weight_out, *later),
+        scratch=[pltpu.VMEM((n_kv, 8, wide), WIDE), pltpu.VMEM((rows, wide), WIDE)],
+        cost_us=COST_OUT,
+    )
+
+
+def up_step(ranks, step, chunk, gain_tiles, weight_up, before):
+    rows, cols = chunk.shape
+    parts = cols // 128
+
+    def kernel(kv_ref, tp_ref, chunk_ref, gain_ref, weight_ref, *refs):
+        start = pl.multiple_of((kv_ref[0] ^ step) * cols, 128)
+        wide = chunk_ref[...].astype(WIDE)
+        tile = pl.multiple_of((kv_ref[0] ^ step) * parts, 8)
+        gain = gain_ref[pl.ds(tile, parts), :].astype(WIDE)
+        scaled = jnp.concatenate(
+            [wide[:, p * 128 : (p + 1) * 128] * gain[p : p + 1, :] for p in range(parts)], axis=1
+        ).astype(NARROW)
+        part = jnp.dot(scaled, weight_ref[pl.ds(start, cols), :], preferred_element_type=WIDE)
+        own = jnp.sum(wide * wide, axis=1, keepdims=True)
+        if before:
+            part = refs[0][...] + part
+            own = refs[1][...] + own
+        refs[-2][...] = part
+        refs[-1][...] = own
+
+    return kernel_call(
+        ranks,
+        kernel,
+        "up_step",
+        [shaped((rows, weight_up.shape[1]), WIDE), shaped((rows, 1), WIDE)],
+        (chunk, gain_tiles, weight_up, *before),
+        limit=4,
+    )
+
+
+def down_half(ranks, other, total, squares, weight_down, n_kv, width_full, dtype):
+    rows = total.shape[0]
+    cols = weight_down.shape[1] // (n_kv * 2)
+
+    def kernel(kv_ref, tp_ref, total_ref, squares_ref, weight_ref, out_ref):
+        inverse = lax.rsqrt(squares_ref[...] / width_full + epsilon)
+        activation = jnp.maximum(inverse * total_ref[...], 0.0)
+        squared = (activation * activation).astype(NARROW)
+        half = tp_ref[0] ^ other
+        for block in range(n_kv):
+            start = pl.multiple_of((block * 2 + half) * cols, 128)
+            out_ref[block] = jnp.dot(
+                squared, weight_ref[:, pl.ds(start, cols)], preferred_element_type=WIDE
+            ).astype(dtype)
+
+    return kernel_call(
+        ranks,
+        kernel,
+        "down_half",
+        shaped((n_kv, rows, cols), dtype),
+        (total, squares, weight_down),
+        limit=4,
+    )
+
+
+def share(ranks, here, got, mixed_slab, n_kv):
+    _, rows, cols = here.shape
+    steps = [step for step, _ in steps_of(n_kv)]
+
+    def kernel(kv_ref, tp_ref, here_ref, got_ref, mixed_ref, own_ref, *outs):
+        kv = kv_ref[0]
+        mixed = jnp.where(tp_ref[0] == 0, mixed_ref[:, :cols].astype(WIDE), mixed_ref[:, cols:].astype(WIDE))
+        own_ref[...] = here_ref[kv] + got_ref[kv].astype(WIDE) + mixed
+        for out, step in zip(outs, steps):
+            out[...] = (here_ref[kv ^ step] + got_ref[kv ^ step].astype(WIDE)).astype(NARROW)
+
+    return kernel_call(
+        ranks,
+        kernel,
+        "share",
+        [shaped((rows, cols), WIDE)] + [shaped((rows, cols), NARROW)] * len(steps),
+        (here, got, mixed_slab),
+    )
+
+
+COST_LOAD = 0
+COST_PACK = 40
+COST_CELL = 0
+COST_OUT = 0
 
 
 def solution(mesh):
@@ -181,6 +509,97 @@
         layer_out = (mixed_own.astype(jnp.float32) + here).astype(jnp.bfloat16)
         return (layer_out, new_memory, new_normalizer, new_stabilizer)
 
+    swap = [(0, 1), (1, 0)]
+
+    def fast_body(
+        tokens,
+        gain_mixer,
+        weight_query,
+        weight_key,
+        weight_value,
+        weight_outgate,
+        weight_ingate,
+        weight_forget,
+        bias_input,
+        bias_forget,
+        memory,
+        normalizer,
+        stabilizer,
+        head_gain,
+        weight_out,
+        gain_channel,
+        weight_up,
+        weight_down,
+    ):
+        ranks = (lax.axis_index("kv").reshape(1), lax.axis_index("tp").reshape(1))
+        heads_here = memory.shape[1]
+        width_full = gain_mixer.shape[0]
+        other = lax.ppermute(tokens, "tp", swap)
+        mine, own_gain, gates, *weights = load_first(
+            ranks,
+            tokens,
+            gain_mixer.reshape(-1, 128),
+            weight_ingate.T,
+            weight_forget.T,
+            (weight_query, weight_key, weight_value, weight_outgate),
+            heads_here,
+            2 * tokens.shape[1],
+        )
+        slab, scaled, extra = start_block(ranks, mine, other, own_gain, gates)
+        partials = [project(scaled, weight) for weight in weights]
+        own, *sends = pack(ranks, partials, extra, n_kv)
+        parts = [own] + [
+            lax.ppermute(send, "kv", pairs) for send, (_, pairs) in zip(sends, steps_of(n_kv))
+        ]
+        heads_out, new_normalizer, new_stabilizer, retain, values_in, keys_scaled = cell(
+            ranks,
+            parts,
+            bias_input.reshape(1, -1),
+            bias_forget.reshape(1, -1),
+            stabilizer,
+            normalizer,
+            head_gain,
+            memory,
+            width_full,
+        )
+        arrived = [lax.ppermute(heads_out, "kv", pairs) for _, pairs in steps_of(n_kv)]
+        new_memory = (
+            retain[..., None, None] * memory + values_in[..., :, None] * keys_scaled[..., None, :]
+        )
+        partial_out = out_step(
+            ranks, heads_out, arrived, weight_out, (weight_up, weight_down), n_kv
+        )
+        partial_other = lax.ppermute(partial_out, "tp", swap)
+        mixed_slab = (
+            slab.astype(jnp.float32)
+            + (partial_out.astype(jnp.float32) + partial_other.astype(jnp.float32))
+        ).astype(jnp.bfloat16)
+        chunks = [(0, mixed_slab)] + [
+            (step, lax.ppermute(mixed_slab, "kv", pairs)) for step, pairs in steps_of(n_kv)
+        ]
+        before = ()
+        for step, chunk in chunks:
+            before = up_step(ranks, step, chunk, gain_channel.reshape(-1, 128), weight_up, before)
+        theirs = down_half(ranks, 1, *before, weight_down, n_kv, width_full, jnp.bfloat16)
+        got = lax.ppermute(theirs, "tp", swap)
+        here = down_half(ranks, 0, *before, weight_down, n_kv, width_full, jnp.float32)
+        own, *sends = share(ranks, here, got, mixed_slab, n_kv)
+        for send, (_, pairs) in zip(sends, steps_of(n_kv)):
+            own = own + lax.ppermute(send, "kv", pairs).astype(jnp.float32)
+        return (own.astype(jnp.bfloat16), new_memory, new_normalizer, new_stabilizer)
+
+    def chosen(tokens, *rest):
+        memory = rest[9]
+        fits = (
+            n_tp == 2
+            and n_kv in (2, 4, 8)
+            and tokens.shape[1] % 512 == 0
+            and memory.shape[0] <= 8
+            and memory.shape[1] == 8
+            and memory.shape[2] == 128
+        )
+        return (fast_body if fits else body)(tokens, *rest)
+
     placed = (
         P("dp", ("kv", "tp")),
         P(),
@@ -202,7 +621,7 @@
         P(("kv", "tp"), None),
     )
     return jax.shard_map(
-        body,
+        chosen,
         mesh=mesh,
         in_specs=placed,
         out_specs=(

time: 73.2 us -> 49.5 us (0.68)
  matrix products: 19.3 us -> 1.58 us
  Pallas kernels: 0 us -> 12.8 us
  local copies, waits for them, and re-layouts: 9.89 us -> 0.09 us
  waiting for transfers between devices: 17 us -> 11.8 us
  other arithmetic: 6.31 us -> 2.82 us
    dot_general x4 -> x0, matrix products: 16 us -> none  [the longest x1 12.9 us: body(): down = jnp.dot(squared, weight_down, preferred_element_type=jnp.float32)]
    pallas_call x0 -> x12, Pallas kernels: none -> 12.8 us  [kernel_call(): pl.pallas_call(kernel, out_shape=outs if single else tuple(outs), in_spec...]
    ppermute x15, waiting for transfers between devices: 17 us -> 11.8 us  [the longest x3 4.7 us: fast_body(): lax.ppermute(send, 'kv', pairs)]
    dynamic_update_slice x11 -> x0, local copies, waits for them, and re-layouts: 4.29 us -> none  [the longest x8 2.83 us: gather_over(): lax.dynamic_update_index_in_dim(whole, got, source_of(rank, step, size), 0)]
    unnamed x29 -> x32, local copies, waits for them, and re-layouts: 3.08 us -> 0.09 us
    dot_general x4, matrix products: 3.28 us -> 1.58 us  [project(): jnp.dot(scaled, weight.reshape(weight.shape[0], -1), preferred_element_ty...]
    reduce_sum x6 -> x0, other arithmetic: 1.58 us -> none  [the longest x1 0.69 us: cell_update(): denominator = jnp.sum(new_normalizer * query_wide, axis=-1)]
    broadcast_in_dim x12 -> x0, local copies, waits for them, and re-layouts: 1.29 us -> none  [the longest x2 0.81 us: gather_over(): whole = lax.dynamic_update_index_in_dim(whole, piece, rank, 0)]
  transfers between devices with their start and end apart: 15 -> 15, of which waited for: 11 -> 8; matrix products, arithmetic and copies ran while one was open for 5% -> 4% of each run, Pallas kernels for 0% -> 16%
where the time goes in v2:
time: 49.5 us; the launch traced here: 49.3 us
  starting transfers between devices  19.3 us (39%)
  Pallas kernels  12.8 us (26%)
  waiting for transfers between devices  11.8 us (24%)
  other arithmetic  2.82 us (6%)
  matrix products  1.58 us (3%)
  between operations  0.91 us (2%)
    pallas_call x12, Pallas kernels, kernel_call(): pl.pallas_call(kernel, out_shape=outs if single else tuple(outs), in_spec...  12.8 us
    ppermute x3, starting transfers between devices, fast_body(): lax.ppermute(send, 'kv', pairs)  5.32 us
    ppermute x3, waiting for transfers between devices, fast_body(): lax.ppermute(send, 'kv', pairs)  4.7 us
    ppermute x3, starting transfers between devices, fast_body(): own = own + lax.ppermute(send, 'kv', pairs).astype(jnp.float32)  4.45 us
    ppermute x3, starting transfers between devices, fast_body(): lax.ppermute(mixed_slab, 'kv', pairs)  4.45 us
    ppermute x3, starting transfers between devices, fast_body(): lax.ppermute(heads_out, 'kv', pairs)  4.45 us
    ppermute x3, waiting for transfers between devices, fast_body(): lax.ppermute(heads_out, 'kv', pairs)  4.07 us
    add x1, other arithmetic, fast_body(): retain[..., None, None] * memory  2.17 us
  transfers between devices with their start and end apart: 15, of which 8 were waited for; matrix products, arithmetic and copies ran while one was open for 4% of the time, Pallas kernels for 16%

profile of v2, /device:TPU:0, one launch (start us, length us, event | category | flops | bytes accessed | tf_op | source)
XLA Modules:
  0.0 49.3 jit_solution(5990257203754906557)
XLA Ops:
  0.6 0.6 %collective-permute-start = (bf16[24,512]{1,0:T(8,128)(2,1)}, bf16[24,512]{1,0:T(8,128)(2,1)S(1)}, u32[]{:S(2)}, u32[]{:S(2)}) collective-permute-start(bf16[24,512]{1,0:T(8,128)(2,1)} %tokens_ref.1), channel_id=1, source_target_pairs={{0,1},{1,0},{2,3},{3,2},{4,5},{5,4},{6,7},{7,6},{8,9},{9,8},{10,11... | collective-permute-start | bytes 73736 | tf_op jit(solution)/shard_map/ppermute | solution.py:537
  1.2 3.6 %load_first.1 = (bf16[24,512]{1,0:T(8,128)(2,1)S(1)}, bf16[8,128]{1,0:T(8,128)(2,1)S(1)}, bf16[16,1024]{1,0:T(8,128)(2,1)S(1)}, bf16[1024,8,128]{2,1,0:T(8,128)(...) custom-call(s32[1]{0:T(128)} %bitcast.kv_ref, ...), custom_call_target="tpu_custom_call" | custom-call | flops 1 | bytes 1 | tf_op jit(solution)/shard_map/load_first/pallas_call | solution.py:96
  4.9 0.4 fusion.refs_3_
  5.3 0.4 fusion.3.refs_2_
  5.7 0.4 fusion.6.refs_1_
  6.1 0.4 fusion.9.refs_0_
  6.8 4.7 %collective-permute-start.1 = (bf16[24,1152]{1,0:T(8,128)(2,1)S(1)}, bf16[24,1152]{1,0:T(8,128)(2,1)S(1)}, u32[]{:S(2)}, u32[]{:S(2)}) collective-permute-start(bf16[24,1152]{1,0:T(8,128)(2,1)S(1)} %get-tuple-element.47), channel_id=1, source_target_pairs={{0,6},{2,4},{4,2},{6,0},{1,7},{3,5},{5,3},{7,1},{8,14},{10,12},{12... | collective-permute-start | bytes 165896 | tf_op jit(solution)/shard_map/ppermute | solution.py:552
  11.5 0.6 %collective-permute-start.3 = (bf16[24,1152]{1,0:T(8,128)(2,1)S(1)}, bf16[24,1152]{1,0:T(8,128)(2,1)S(1)}, u32[]{:S(2)}, u32[]{:S(2)}) collective-permute-start(bf16[24,1152]{1,0:T(8,128)(2,1)S(1)} %get-tuple-element.49), channel_id=1, source_target_pairs={{0,2},{2,0},{4,6},{6,4},{1,3},{3,1},{5,7},{7,5},{8,10},{10,8},{12,... | collective-permute-start | bytes 165896 | tf_op jit(solution)/shard_map/ppermute | solution.py:552
  12.1 2.0 %collective-permute-done.1.refs_1_ = bf16[24,1152]{1,0:T(8,128)(2,1)S(1)} collective-permute-done((bf16[24,1152]{1,0:T(8,128)(2,1)S(1)}, bf16[24,1152]{1,0:T(8,128)(2,1)S(1)}, u32[]{:S(2)}, u32[]{:S(2)}) %collective-permute-start.1) | collective-permute-done | bytes 55328 | tf_op jit(solution)/shard_map/ppermute | solution.py:552
  14.1 2.7 %collective-permute-done.2.refs_2_ = bf16[24,1152]{1,0:T(8,128)(2,1)S(1)} collective-permute-done((bf16[24,1152]{1,0:T(8,128)(2,1)S(1)}, bf16[24,1152]{1,0:T(8,128)(2,1)S(1)}, u32[]{:S(2)}, u32[]{:S(2)}) %collective-permute-start.2) | collective-permute-done | bytes 55328 | tf_op jit(solution)/shard_map/ppermute | solution.py:552
  16.9 2.0 %cell.1 = (bf16[6,1024]{1,0:T(8,128)(2,1)S(1)}, f32[6,8,128]{2,1,0:T(8,128)}, f32[6,8]{1,0:T(8,128)}, f32[6,8]{1,0:T(8,128)S(1)}, f32[6,8,128]{2,1,0:T(8,128)S(1)}, /*index=5*/f32[6,8,128]{2,1,0:T(8,128)S(1)}) custom-call(s32[1]{0:T(128)} %bitcast.kv_ref, s32[1]{0:T(128)} %bitcast.1.tp_ref, f32[24,1152]{1,0:T(8,128)S(1)} %get-tuple-element.46.refs_0_, ...), custom_call_target="tpu_custom_call" | custom-call | flops 1 | bytes 1 | tf_op jit(solution)/shard_map/cell/pallas_call | solution.py:96
  18.9 1.4 %collective-permute-start.6 = (bf16[6,1024]{1,0:T(8,128)(2,1)S(1)}, bf16[6,1024]{1,0:T(8,128)(2,1)S(1)}, u32[]{:S(2)}, u32[]{:S(2)}) collective-permute-start(bf16[6,1024]{1,0:T(8,128)(2,1)S(1)} %get-tuple-element.50.own_ref), channel_id=1, source_target_pairs={{0,2},{2,0},{4,6},{6,4},{1,3},{3,1},{5,7},{7,5},{8,10},{10,8},{12,... | collective-permute-start | bytes 36872 | tf_op jit(solution)/shard_map/ppermute | solution.py:565
  20.3 1.6 %collective-permute-start.5 = (bf16[6,1024]{1,0:T(8,128)(2,1)S(1)}, bf16[6,1024]{1,0:T(8,128)(2,1)S(1)}, u32[]{:S(2)}, u32[]{:S(2)}) collective-permute-start(bf16[6,1024]{1,0:T(8,128)(2,1)S(1)} %get-tuple-element.50.own_ref), channel_id=1, source_target_pairs={{0,4},{2,6},{4,0},{6,2},{1,5},{3,7},{5,1},{7,3},{8,12},{10,14},{12... | collective-permute-start | bytes 36872 | tf_op jit(solution)/shard_map/ppermute | solution.py:565
  21.9 1.5 %collective-permute-start.4 = (bf16[6,1024]{1,0:T(8,128)(2,1)S(1)}, bf16[6,1024]{1,0:T(8,128)(2,1)S(1)}, u32[]{:S(2)}, u32[]{:S(2)}) collective-permute-start(bf16[6,1024]{1,0:T(8,128)(2,1)S(1)} %get-tuple-element.50.own_ref), channel_id=1, source_target_pairs={{0,6},{2,4},{4,2},{6,0},{1,7},{3,5},{5,3},{7,1},{8,14},{10,12},{12... | collective-permute-start | bytes 36872 | tf_op jit(solution)/shard_map/ppermute | solution.py:565
  23.3 1.6 %collective-permute-done.5.refs_1_ = bf16[6,1024]{1,0:T(8,128)(2,1)S(1)} collective-permute-done((bf16[6,1024]{1,0:T(8,128)(2,1)S(1)}, bf16[6,1024]{1,0:T(8,128)(2,1)S(1)}, u32[]{:S(2)}, u32[]{:S(2)}) %collective-permute-start.5) | collective-permute-done | bytes 12320 | tf_op jit(solution)/shard_map/ppermute | solution.py:565
  24.9 2.5 %collective-permute-done.4.refs_0_ = bf16[6,1024]{1,0:T(8,128)(2,1)S(1)} collective-permute-done((bf16[6,1024]{1,0:T(8,128)(2,1)S(1)}, bf16[6,1024]{1,0:T(8,128)(2,1)S(1)}, u32[]{:S(2)}, u32[]{:S(2)}) %collective-permute-start.4) | collective-permute-done | bytes 12320 | tf_op jit(solution)/shard_map/ppermute | solution.py:565
  27.5 0.5 out_step.1
  28.0 1.2 %collective-permute-done.7 = bf16[24,1024]{1,0:T(8,128)(2,1)S(1)} collective-permute-done((bf16[24,1024]{1,0:T(8,128)(2,1)S(1)}, bf16[24,1024]{1,0:T(8,128)(2,1)S(1)}, u32[]{:S(2)}, u32[]{:S(2)}) %collective-permute-start.7) | collective-permute-done | bytes 49184 | tf_op jit(solution)/shard_map/ppermute | solution.py:572
  29.2 1.5 %collective-permute-start.10 = (bf16[24,1024]{1,0:T(8,128)(2,1)S(1)}, bf16[24,1024]{1,0:T(8,128)(2,1)S(1)}, u32[]{:S(2)}, u32[]{:S(2)}) collective-permute-start(bf16[24,1024]{1,0:T(8,128)(2,1)S(1)} %add_convert_fusion.chunk_ref.mixed_ref), channel_id=1, source_target_pairs={{0,6},{2,4},{4,2},{6,0},{1,7},{3,5},{5,3},{7,1},{8,14},{10,12},{12... | collective-permute-start | bytes 147464 | tf_op jit(solution)/shard_map/ppermute | solution.py:578
  30.8 2.9 %collective-permute-start.8 = (bf16[24,1024]{1,0:T(8,128)(2,1)S(1)}, bf16[24,1024]{1,0:T(8,128)(2,1)S(1)}, u32[]{:S(2)}, u32[]{:S(2)}) collective-permute-start(bf16[24,1024]{1,0:T(8,128)(2,1)S(1)} %add_convert_fusion.chunk_ref.mixed_ref), channel_id=1, source_target_pairs={{0,2},{2,0},{4,6},{6,4},{1,3},{3,1},{5,7},{7,5},{8,10},{10,8},{12,... | collective-permute-start | bytes 147464 | tf_op jit(solution)/shard_map/ppermute | solution.py:578
  33.7 0.8 %up_step.4 = (f32[24,2048]{1,0:T(8,128)S(1)}, f32[24,1]{1,0:T(8,128)S(1)}) custom-call(s32[1]{0:T(128)} %bitcast.kv_ref, s32[1]{0:T(128)} %bitcast.1.tp_ref, bf16[24,1024]{1,0:T(8,128)(2,1)S(1)} %add_convert_fusion.chunk_ref.mixed_ref, bf16[32,128]{1,0:T(8,128)(2,1)S(1)} %bitcast.36, bf16[4096,2048]{1,0:T(8,128)(2,1)S(1)} %bitcast.29), custom_call_target="tpu_custom_call" | custom-call | flops 1 | bytes 1 | tf_op jit(solution)/shard_map/up_step/pallas_call | solution.py:96
  34.5 1.0 %collective-permute-done.10.chunk_ref = bf16[24,1024]{1,0:T(8,128)(2,1)S(1)} collective-permute-done((bf16[24,1024]{1,0:T(8,128)(2,1)S(1)}, bf16[24,1024]{1,0:T(8,128)(2,1)S(1)}, u32[]{:S(2)}, u32[]{:S(2)}) %collective-permute-start.10) | collective-permute-done | bytes 49184 | tf_op jit(solution)/shard_map/ppermute | solution.py:578
  35.5 0.8 %up_step.5 = (f32[24,2048]{1,0:T(8,128)S(1)}, f32[24,1]{1,0:T(8,128)S(1)}) custom-call(s32[1]{0:T(128)} %bitcast.kv_ref, s32[1]{0:T(128)} %bitcast.1.tp_ref, bf16[24,1024]{1,0:T(8,128)(2,1)S(1)} %collective-permute-done.10.chunk_ref, bf16[32,128]{1,0:T(8,128)(2,1)S(1)} %bitcast.37, bf16[4096,2048]{1,0:T(8,128)(2,1)S(1)} %bitcast.29, ...), custom_call_target="tpu_custom_call" | custom-call | flops 1 | bytes 1 | tf_op jit(solution)/shard_map/up_step/pallas_call | solution.py:96
  36.4 0.6 %collective-permute-done.9.chunk_ref = bf16[24,1024]{1,0:T(8,128)(2,1)S(1)} collective-permute-done((bf16[24,1024]{1,0:T(8,128)(2,1)S(1)}, bf16[24,1024]{1,0:T(8,128)(2,1)S(1)}, u32[]{:S(2)}, u32[]{:S(2)}) %collective-permute-start.9) | collective-permute-done | bytes 49184 | tf_op jit(solution)/shard_map/ppermute | solution.py:578
  37.0 0.8 %up_step.6 = (f32[24,2048]{1,0:T(8,128)S(1)}, f32[24,1]{1,0:T(8,128)S(1)}) custom-call(s32[1]{0:T(128)} %bitcast.kv_ref, s32[1]{0:T(128)} %bitcast.1.tp_ref, bf16[24,1024]{1,0:T(8,128)(2,1)S(1)} %collective-permute-done.9.chunk_ref, bf16[32,128]{1,0:T(8,128)(2,1)S(1)} %bitcast.38, bf16[4096,2048]{1,0:T(8,128)(2,1)S(1)} %bitcast.29, ...), custom_call_target="tpu_custom_call" | custom-call | flops 1 | bytes 1 | tf_op jit(solution)/shard_map/up_step/pallas_call | solution.py:96
  37.9 0.8 %up_step.7 = (f32[24,2048]{1,0:T(8,128)S(1)}, f32[24,1]{1,0:T(8,128)S(1)}) custom-call(s32[1]{0:T(128)} %bitcast.kv_ref, s32[1]{0:T(128)} %bitcast.1.tp_ref, bf16[24,1024]{1,0:T(8,128)(2,1)S(1)} %collective-permute-done.8.chunk_ref, bf16[32,128]{1,0:T(8,128)(2,1)S(1)} %bitcast.39, bf16[4096,2048]{1,0:T(8,128)(2,1)S(1)} %bitcast.29, ...), custom_call_target="tpu_custom_call" | custom-call | flops 1 | bytes 1 | tf_op jit(solution)/shard_map/up_step/pallas_call | solution.py:96
  38.7 1.6 %down_half.3 = bf16[4,24,512]{2,1,0:T(8,128)(2,1)S(1)} custom-call(s32[1]{0:T(128)} %bitcast.kv_ref, s32[1]{0:T(128)} %bitcast.1.tp_ref, f32[24,2048]{1,0:T(8,128)S(1)} %get-tuple-element.57.total_ref, f32[24,1]{1,0:T(8,128)S(1)} %get-tuple-element.58.squares_ref, bf16[2048,4096]{1,0:T(8,128)(2,1)S(1)} %bitcast.31), custom_call_target="tpu_custom_call" | custom-call | flops 1 | bytes 1 | tf_op jit(solution)/shard_map/down_half/pallas_call | solution.py:96
  40.3 1.6 %down_half.2.here_ref = f32[4,24,512]{2,1,0:T(8,128)S(1)} custom-call(s32[1]{0:T(128)} %bitcast.kv_ref, s32[1]{0:T(128)} %bitcast.1.tp_ref, f32[24,2048]{1,0:T(8,128)S(1)} %get-tuple-element.57.total_ref, f32[24,1]{1,0:T(8,128)S(1)} %get-tuple-element.58.squares_ref, bf16[2048,4096]{1,0:T(8,128)(2,1)S(1)} %bitcast.31), custom_call_target="tpu_custom_call" | custom-call | flops 1 | bytes 1 | tf_op jit(solution)/shard_map/down_half/pallas_call | solution.py:96
  42.0 1.5 %collective-permute-start.12 = (bf16[24,512]{1,0:T(8,128)(2,1)S(1)}, bf16[24,512]{1,0:T(8,128)(2,1)S(1)}, u32[]{:S(2)}, u32[]{:S(2)}) collective-permute-start(bf16[24,512]{1,0:T(8,128)(2,1)S(1)} %get-tuple-element.60), channel_id=1, source_target_pairs={{0,6},{2,4},{4,2},{6,0},{1,7},{3,5},{5,3},{7,1},{8,14},{10,12},{12... | collective-permute-start | bytes 73736 | tf_op jit(solution)/shard_map/ppermute | solution.py:588
  43.5 2.9 %collective-permute-start.14 = (bf16[24,512]{1,0:T(8,128)(2,1)S(1)}, bf16[24,512]{1,0:T(8,128)(2,1)S(1)}, u32[]{:S(2)}, u32[]{:S(2)}) collective-permute-start(bf16[24,512]{1,0:T(8,128)(2,1)S(1)} %get-tuple-element.62), channel_id=1, source_target_pairs={{0,2},{2,0},{4,6},{6,4},{1,3},{3,1},{5,7},{7,5},{8,10},{10,8},{12,... | collective-permute-start | bytes 73736 | tf_op jit(solution)/shard_map/ppermute | solution.py:588
  46.4 2.2 %multiply_add_fusion = f32[6,8,128,128]{3,2,1,0:T(8,128)} fusion(f32[6,8,128,128]{3,2,1,0:T(8,128)S(1)} %copy-done, f32[6,8,128]{2,1,0:T(8,128)S(1)} %get-tuple-element.65, f32[6,8,128]{2,1,0:T(8,128)S(1)} %get-tuple-element.64, f32[6,8]{1,0:T(8,128)S(1)} %get-tuple-element.63), kind=kLoop, calls=%fused_computation | loop fusion | flops 2359296 | bytes 6340800 | tf_op jit(solution)/shard_map/add | solution.py:567
  48.7 0.6 %add_convert_fusion.1 = bf16[24,512]{1,0:T(8,128)(2,1)} fusion(bf16[24,512]{1,0:T(8,128)(2,1)S(1)} %collective-permute-done.14, bf16[24,512]{1,0:T(8,128)(2,1)S(1)} %collective-permute-done.13, f32[24,512]{1,0:T(8,128)S(1)} %get-tuple-element.59, bf16[24,512]{1,0:T(8,128)(2,1)S(1)} %collective-permute-done.12), kind=kLoop, calls=%fused_computation.14 | loop fusion | flops 86016 | bytes 147456 | tf_op jit(solution)/shard_map/convert_element_type | solution.py:589
  (51 shorter events, 0.6 us)
Async XLA Ops:
  0.6 4.2 %collective-permute-start = (bf16[24,512]{1,0:T(8,128)(2,1)}, bf16[24,512]{1,0:T(8,128)(2,1)S(1)}, u32[]{:S(2)}, u32[]{:S(2)}) collective-permute-start(bf16[24,512]{1,0:T(8,128)(2,1)} %tokens_ref.1), channel_id=1, source_target_pairs={{0,1},{1,0},{2,3},{3,2},{4,5},{5,4},{6,7},{7,6},{8,9},{9,8},{10,11... | collective-permute-start | bytes 73736 | tf_op jit(solution)/shard_map/ppermute | solution.py:537
  6.5 20.9 %slice-start = ((s8[16777216]{0:T(1024)(128)(4,1)}), s8[4194304]{0:T(1024)(128)(4,1)S(1)}, s32[]{:S(2)}) async-start(s8[16777216]{0:T(1024)(128)(4,1)} %bitcast.28), calls=%async_computation | async-start | bytes 8388608
  6.5 20.9 %slice-start.4 = ((s8[16777216]{0:T(1024)(128)(4,1)}), s8[4194304]{0:T(1024)(128)(4,1)S(1)}, s32[]{:S(2)}) async-start(s8[16777216]{0:T(1024)(128)(4,1)} %bitcast.30), calls=%async_computation.4 | async-start | bytes 8388608
  6.5 10.3 %copy-start = (f32[6,8,128,128]{3,2,1,0:T(8,128)S(1)}, f32[6,8,128,128]{3,2,1,0:T(8,128)}, u32[]{:S(2)}) copy-start(f32[6,8,128,128]{3,2,1,0:T(8,128)} %refs_9_.1) | copy-start | bytes 9437188
  6.5 10.3 %copy-start.3 = (f32[6,8,128]{2,1,0:T(8,128)S(1)}, f32[6,8,128]{2,1,0:T(8,128)}, u32[]{:S(2)}) copy-start(f32[6,8,128]{2,1,0:T(8,128)} %refs_7_.1) | copy-start | bytes 73732
  6.6 10.3 %copy-start.4 = (f32[6,8]{1,0:T(8,128)S(1)}, f32[6,8]{1,0:T(8,128)}, u32[]{:S(2)}) copy-start(f32[6,8]{1,0:T(8,128)} %refs_6_.1) | copy-start | bytes 580
  6.6 10.3 %copy-start.5 = (bf16[16,128]{1,0:T(8,128)(2,1)S(1)}, bf16[16,128]{1,0:T(8,128)(2,1)}, u32[]{:S(2)}) copy-start(bf16[16,128]{1,0:T(8,128)(2,1)} %refs_8_.1) | copy-start | bytes 12292
  6.6 10.3 %copy-start.6 = (f32[16]{0:T(128)S(1)}, f32[16]{0:T(128)}, u32[]{:S(2)}) copy-start(f32[16]{0:T(128)} %param.26) | copy-start | bytes 196
  6.6 10.3 %copy-start.7 = (f32[16]{0:T(128)S(1)}, f32[16]{0:T(128)}, u32[]{:S(2)}) copy-start(f32[16]{0:T(128)} %param.27) | copy-start | bytes 196
  6.6 20.8 %slice-start.1 = ((s8[16777216]{0:T(1024)(128)(4,1)}), s8[4194304]{0:T(1024)(128)(4,1)S(1)}, s32[]{:S(2)}) async-start(s8[16777216]{0:T(1024)(128)(4,1)} %bitcast.28), calls=%async_computation.1 | async-start | bytes 8388608
  6.6 20.8 %slice-start.2 = ((s8[16777216]{0:T(1024)(128)(4,1)}), s8[4194304]{0:T(1024)(128)(4,1)S(1)}, s32[]{:S(2)}) async-start(s8[16777216]{0:T(1024)(128)(4,1)} %bitcast.28), calls=%async_computation.2 | async-start | bytes 8388608
  6.6 20.8 %slice-start.3 = ((s8[16777216]{0:T(1024)(128)(4,1)}), s8[4194304]{0:T(1024)(128)(4,1)S(1)}, s32[]{:S(2)}) async-start(s8[16777216]{0:T(1024)(128)(4,1)} %bitcast.28), calls=%async_computation.3 | async-start | bytes 8388608
  6.6 20.8 %slice-start.5 = ((s8[16777216]{0:T(1024)(128)(4,1)}), s8[4194304]{0:T(1024)(128)(4,1)S(1)}, s32[]{:S(2)}) async-start(s8[16777216]{0:T(1024)(128)(4,1)} %bitcast.30), calls=%async_computation.5 | async-start | bytes 8388608
  6.7 20.8 %slice-start.6 = ((s8[16777216]{0:T(1024)(128)(4,1)}), s8[4194304]{0:T(1024)(128)(4,1)S(1)}, s32[]{:S(2)}) async-start(s8[16777216]{0:T(1024)(128)(4,1)} %bitcast.30), calls=%async_computation.6 | async-start | bytes 8388608
  6.7 20.8 %slice-start.7 = ((s8[16777216]{0:T(1024)(128)(4,1)}), s8[4194304]{0:T(1024)(128)(4,1)S(1)}, s32[]{:S(2)}) async-start(s8[16777216]{0:T(1024)(128)(4,1)} %bitcast.30), calls=%async_computation.7 | async-start | bytes 8388608
  6.8 20.7 %copy-start.1 = (bf16[1024,1024]{1,0:T(8,128)(2,1)S(1)}, bf16[1024,1024]{1,0:T(8,128)(2,1)}, u32[]{:S(2)}) copy-start(bf16[1024,1024]{1,0:T(8,128)(2,1)} %refs_3_.3) | copy-start | bytes 6291460
  6.8 7.3 %collective-permute-start.1 = (bf16[24,1152]{1,0:T(8,128)(2,1)S(1)}, bf16[24,1152]{1,0:T(8,128)(2,1)S(1)}, u32[]{:S(2)}, u32[]{:S(2)}) collective-permute-start(bf16[24,1152]{1,0:T(8,128)(2,1)S(1)} %get-tuple-element.47), channel_id=1, source_target_pairs={{0,6},{2,4},{4,2},{6,0},{1,7},{3,5},{5,3},{7,1},{8,14},{10,12},{12... | collective-permute-start | bytes 165896 | tf_op jit(solution)/shard_map/ppermute | solution.py:552
  11.5 5.3 %collective-permute-start.2 = (bf16[24,1152]{1,0:T(8,128)(2,1)S(1)}, bf16[24,1152]{1,0:T(8,128)(2,1)S(1)}, u32[]{:S(2)}, u32[]{:S(2)}) collective-permute-start(bf16[24,1152]{1,0:T(8,128)(2,1)S(1)} %get-tuple-element.48), channel_id=1, source_target_pairs={{0,4},{2,6},{4,0},{6,2},{1,5},{3,7},{5,1},{7,3},{8,12},{10,14},{12... | collective-permute-start | bytes 165896 | tf_op jit(solution)/shard_map/ppermute | solution.py:552
  11.5 5.3 %collective-permute-start.3 = (bf16[24,1152]{1,0:T(8,128)(2,1)S(1)}, bf16[24,1152]{1,0:T(8,128)(2,1)S(1)}, u32[]{:S(2)}, u32[]{:S(2)}) collective-permute-start(bf16[24,1152]{1,0:T(8,128)(2,1)S(1)} %get-tuple-element.49), channel_id=1, source_target_pairs={{0,2},{2,0},{4,6},{6,4},{1,3},{3,1},{5,7},{7,5},{8,10},{10,8},{12,... | collective-permute-start | bytes 165896 | tf_op jit(solution)/shard_map/ppermute | solution.py:552
  18.9 14.8 %copy-start.2 = (bf16[4096]{0:T(1024)(128)(2,1)S(1)}, bf16[4096]{0:T(1024)(128)(2,1)}, u32[]{:S(2)}) copy-start(bf16[4096]{0:T(1024)(128)(2,1)} %param.33) | copy-start | bytes 24580
  18.9 4.5 %collective-permute-start.6 = (bf16[6,1024]{1,0:T(8,128)(2,1)S(1)}, bf16[6,1024]{1,0:T(8,128)(2,1)S(1)}, u32[]{:S(2)}, u32[]{:S(2)}) collective-permute-start(bf16[6,1024]{1,0:T(8,128)(2,1)S(1)} %get-tuple-element.50.own_ref), channel_id=1, source_target_pairs={{0,2},{2,0},{4,6},{6,4},{1,3},{3,1},{5,7},{7,5},{8,10},{10,8},{12,... | collective-permute-start | bytes 36872 | tf_op jit(solution)/shard_map/ppermute | solution.py:565
  20.3 4.6 %collective-permute-start.5 = (bf16[6,1024]{1,0:T(8,128)(2,1)S(1)}, bf16[6,1024]{1,0:T(8,128)(2,1)S(1)}, u32[]{:S(2)}, u32[]{:S(2)}) collective-permute-start(bf16[6,1024]{1,0:T(8,128)(2,1)S(1)} %get-tuple-element.50.own_ref), channel_id=1, source_target_pairs={{0,4},{2,6},{4,0},{6,2},{1,5},{3,7},{5,1},{7,3},{8,12},{10,14},{12... | collective-permute-start | bytes 36872 | tf_op jit(solution)/shard_map/ppermute | solution.py:565
  21.9 5.5 %collective-permute-start.4 = (bf16[6,1024]{1,0:T(8,128)(2,1)S(1)}, bf16[6,1024]{1,0:T(8,128)(2,1)S(1)}, u32[]{:S(2)}, u32[]{:S(2)}) collective-permute-start(bf16[6,1024]{1,0:T(8,128)(2,1)S(1)} %get-tuple-element.50.own_ref), channel_id=1, source_target_pairs={{0,6},{2,4},{4,2},{6,0},{1,7},{3,5},{5,3},{7,1},{8,14},{10,12},{12... | collective-permute-start | bytes 36872 | tf_op jit(solution)/shard_map/ppermute | solution.py:565
  28.0 1.2 %collective-permute-start.7 = (bf16[24,1024]{1,0:T(8,128)(2,1)S(1)}, bf16[24,1024]{1,0:T(8,128)(2,1)S(1)}, u32[]{:S(2)}, u32[]{:S(2)}) collective-permute-start(bf16[24,1024]{1,0:T(8,128)(2,1)S(1)} %out_step.1), channel_id=1, source_target_pairs={{0,1},{1,0},{2,3},{3,2},{4,5},{5,4},{6,7},{7,6},{8,9},{9,8},{10,11... | collective-permute-start | bytes 147464 | tf_op jit(solution)/shard_map/ppermute | solution.py:572
  29.2 6.3 %collective-permute-start.10 = (bf16[24,1024]{1,0:T(8,128)(2,1)S(1)}, bf16[24,1024]{1,0:T(8,128)(2,1)S(1)}, u32[]{:S(2)}, u32[]{:S(2)}) collective-permute-start(bf16[24,1024]{1,0:T(8,128)(2,1)S(1)} %add_convert_fusion.chunk_ref.mixed_ref), channel_id=1, source_target_pairs={{0,6},{2,4},{4,2},{6,0},{1,7},{3,5},{5,3},{7,1},{8,14},{10,12},{12... | collective-permute-start | bytes 147464 | tf_op jit(solution)/shard_map/ppermute | solution.py:578
  30.8 6.2 %collective-permute-start.9 = (bf16[24,1024]{1,0:T(8,128)(2,1)S(1)}, bf16[24,1024]{1,0:T(8,128)(2,1)S(1)}, u32[]{:S(2)}, u32[]{:S(2)}) collective-permute-start(bf16[24,1024]{1,0:T(8,128)(2,1)S(1)} %add_convert_fusion.chunk_ref.mixed_ref), channel_id=1, source_target_pairs={{0,4},{2,6},{4,0},{6,2},{1,5},{3,7},{5,1},{7,3},{8,12},{10,14},{12... | collective-permute-start | bytes 147464 | tf_op jit(solution)/shard_map/ppermute | solution.py:578
  30.8 7.1 %collective-permute-start.8 = (bf16[24,1024]{1,0:T(8,128)(2,1)S(1)}, bf16[24,1024]{1,0:T(8,128)(2,1)S(1)}, u32[]{:S(2)}, u32[]{:S(2)}) collective-permute-start(bf16[24,1024]{1,0:T(8,128)(2,1)S(1)} %add_convert_fusion.chunk_ref.mixed_ref), channel_id=1, source_target_pairs={{0,2},{2,0},{4,6},{6,4},{1,3},{3,1},{5,7},{7,5},{8,10},{10,8},{12,... | collective-permute-start | bytes 147464 | tf_op jit(solution)/shard_map/ppermute | solution.py:578
  40.3 1.6 %collective-permute-start.11 = (bf16[4,24,512]{2,1,0:T(8,128)(2,1)S(1)}, bf16[4,24,512]{2,1,0:T(8,128)(2,1)S(1)}, u32[]{:S(2)}, u32[]{:S(2)}) collective-permute-start(bf16[4,24,512]{2,1,0:T(8,128)(2,1)S(1)} %down_half.3), channel_id=1, source_target_pairs={{0,1},{1,0},{2,3},{3,2},{4,5},{5,4},{6,7},{7,6},{8,9},{9,8},{10,11... | collective-permute-start | bytes 294920 | tf_op jit(solution)/shard_map/ppermute | solution.py:584
  42.0 6.6 %collective-permute-start.12 = (bf16[24,512]{1,0:T(8,128)(2,1)S(1)}, bf16[24,512]{1,0:T(8,128)(2,1)S(1)}, u32[]{:S(2)}, u32[]{:S(2)}) collective-permute-start(bf16[24,512]{1,0:T(8,128)(2,1)S(1)} %get-tuple-element.60), channel_id=1, source_target_pairs={{0,6},{2,4},{4,2},{6,0},{1,7},{3,5},{5,3},{7,1},{8,14},{10,12},{12... | collective-permute-start | bytes 73736 | tf_op jit(solution)/shard_map/ppermute | solution.py:588
  43.5 5.1 %collective-permute-start.13 = (bf16[24,512]{1,0:T(8,128)(2,1)S(1)}, bf16[24,512]{1,0:T(8,128)(2,1)S(1)}, u32[]{:S(2)}, u32[]{:S(2)}) collective-permute-start(bf16[24,512]{1,0:T(8,128)(2,1)S(1)} %get-tuple-element.61), channel_id=1, source_target_pairs={{0,4},{2,6},{4,0},{6,2},{1,5},{3,7},{5,1},{7,3},{8,12},{10,14},{12... | collective-permute-start | bytes 73736 | tf_op jit(solution)/shard_map/ppermute | solution.py:588
  43.5 5.2 %collective-permute-start.14 = (bf16[24,512]{1,0:T(8,128)(2,1)S(1)}, bf16[24,512]{1,0:T(8,128)(2,1)S(1)}, u32[]{:S(2)}, u32[]{:S(2)}) collective-permute-start(bf16[24,512]{1,0:T(8,128)(2,1)S(1)} %get-tuple-element.62), channel_id=1, source_target_pairs={{0,2},{2,0},{4,6},{6,4},{1,3},{3,1},{5,7},{7,5},{8,10},{10,8},{12,... | collective-permute-start | bytes 73736 | tf_op jit(solution)/shard_map/ppermute | solution.py:588
